TPU v7x, 1024 devices: a 2x16x16 block of a 4x16x16 slice. The times are simulated.
1024 devices in a mesh: grp: 2 (over x), row: 16 (over z), col: 32 (over y, core).
Axes of the slice: x: 2, y: 16, z: 16, core: 2. Of those that a mesh axis runs over, the one named last changes fastest.
The devices are a block of a 4x16x16 slice.
Arguments:
- tokens: bfloat16 [2, 65536, 2048], P('grp', ('row', 'col')), parts along dimension 0, may hold values from -6 to 6
- norm_gain: bfloat16 [2048], replicated, may hold values from 0.099609375 to 1.8984375
- w_in: bfloat16 [2048, 512], replicated, may hold values from -0.125 to 0.125
- w_out: bfloat16 [512, 2048], replicated, may hold values from -0.25 to 0.25
Outputs:
- mixed: bfloat16 [2, 65536, 2048], P('grp', ('row', 'col')), parts along dimension 0
There are 2 independent parts, one for each index of `grp`. A program takes and returns all parts, laid end to end along the dimension named above; an argument that names none is the same for every part. Nothing has to cross between parts.
All inputs are finite; a program needn't handle non-finite values.
Results may differ from a plain program's by a relative error of at most 0.013.
Values may be sent and summed in bfloat16 or wider, within the bound.
No kernel may reach another device: no remote copies, remote signals or barrier semaphores. Data moves between devices by JAX's collectives and lax.ppermute only.
A program may use at most 32 MiB of HBM per device.

v0:
```python
import math

import jax
import jax.numpy as jnp
from jax import lax
from jax.sharding import PartitionSpec as P

GROUP_CH = 128


TWO_PI = 2.0 * math.pi
NORM_EPS = 1e-06


def side_by_side(arrays, axis, split_dim, concat_dim, along):
    widths = [a.shape[along] for a in arrays]
    both = jnp.concatenate(arrays, axis=along)
    filled = lax.all_to_all(both, axis, split_axis=split_dim, concat_axis=concat_dim, tiled=True)
    return tuple(jnp.split(filled, [sum(widths[:k]) for k in range(1, len(widths))], axis=along))


def phase_tables(rows, cols, period):
    left = lax.broadcasted_iota(jnp.int32, (rows, cols), 0)
    right = lax.broadcasted_iota(jnp.int32, (rows, cols), 1)
    angles = (left * right % period).astype(jnp.float32) * (TWO_PI / period)
    return (jnp.cos(angles), jnp.sin(angles))


def rotate_by(pattern, cos_table, sin_table, real_part, imag_part):

    def apply(table, data):
        return jnp.einsum(pattern, table, data)

    return (
        apply(cos_table, real_part) + apply(sin_table, imag_part),
        apply(cos_table, imag_part) - apply(sin_table, real_part),
    )


def twist(real_part, imag_part, cos_table, sin_table):
    return (
        real_part * cos_table + imag_part * sin_table,
        imag_part * cos_table - real_part * sin_table,
    )


def shards(tokens, norm_gain, w_in, w_out):
    seq_count, tok_count, width = tokens.shape
    feat_count = w_in.shape[1]
    row_count = lax.axis_size("row")
    col_count = lax.axis_size("col")
    block_len = tok_count * col_count
    length = block_len * row_count
    sub_feats = feat_count // row_count
    fine_count = tok_count // row_count
    item_count = seq_count * feat_count // col_count
    ortho_scale = 1.0 / math.sqrt(length * GROUP_CH)
    widened = tokens.astype(jnp.float32)
    factor = lax.rsqrt(jnp.mean(widened * widened, -1, keepdims=True) + NORM_EPS)
    normed = (widened * factor * norm_gain.astype(jnp.float32)).astype(jnp.bfloat16)
    mixin = jnp.einsum("std,df->sft", normed, w_in, preferred_element_type=jnp.float32).astype(
        jnp.bfloat16
    )
    row_cos, row_sin = phase_tables(row_count, row_count, row_count)
    chan_cos, chan_sin = phase_tables(GROUP_CH, GROUP_CH, GROUP_CH)
    stacked_shape = (seq_count, sub_feats, row_count, tok_count)
    grouped = mixin.astype(jnp.float32).reshape(
        seq_count, feat_count // GROUP_CH, GROUP_CH, tok_count
    )
    spec_real = jnp.einsum("sgqt,qm->sgmt", grouped, chan_cos).reshape(
        seq_count, feat_count, tok_count
    )
    spec_imag = -jnp.einsum("sgqt,qm->sgmt", grouped, chan_sin).reshape(
        seq_count, feat_count, tok_count
    )
    arrived = tuple(
        (
            part.astype(jnp.float32)
            for part in side_by_side(
                (spec_real.astype(jnp.bfloat16), spec_imag.astype(jnp.bfloat16)), "row", 1, 2, 0
            )
        )
    )
    stacked_real = arrived[0].reshape(stacked_shape)
    stacked_imag = arrived[1].reshape(stacked_shape)
    real_part, imag_part = rotate_by("ka,sfat->skft", row_cos, row_sin, stacked_real, stacked_imag)
    freq_low = lax.broadcasted_iota(jnp.int32, (row_count, tok_count), 0)
    place = lax.axis_index("col") * tok_count + lax.broadcasted_iota(
        jnp.int32, (row_count, tok_count), 1
    )
    angles = (freq_low * place % length).astype(jnp.float32) * (TWO_PI / length)
    real_part, imag_part = twist(
        real_part, imag_part, jnp.cos(angles)[None, :, None, :], jnp.sin(angles)[None, :, None, :]
    )
    sending = (
        real_part.reshape(item_count, col_count, 1, tok_count),
        imag_part.reshape(item_count, col_count, 1, tok_count),
    )
    col_cos, col_sin = phase_tables(col_count, col_count, col_count)
    mid_cos, mid_sin = phase_tables(col_count, tok_count, block_len)
    tok_cos, tok_sin = phase_tables(tok_count, tok_count, tok_count)
    tok_cos = tok_cos.reshape(row_count, fine_count, tok_count)
    tok_sin = tok_sin.reshape(row_count, fine_count, tok_count)
    span_real, span_imag = rotate_by(
        "uc,qct->qut",
        col_cos,
        col_sin,
        lax.all_to_all(
            sending[0].astype(jnp.bfloat16), "col", split_axis=1, concat_axis=2, tiled=True
        ).astype(jnp.float32)[:, 0],
        lax.all_to_all(
            sending[1].astype(jnp.bfloat16), "col", split_axis=1, concat_axis=2, tiled=True
        ).astype(jnp.float32)[:, 0],
    )
    span_real, span_imag = twist(span_real, span_imag, mid_cos, mid_sin)
    span_real, span_imag = rotate_by("rjt,qut->rjuq", tok_cos, tok_sin, span_real, span_imag)
    owner_shape = (row_count, col_count, fine_count, span_real.shape[-1], 1)
    span_real, span_imag = (span_real.reshape(owner_shape), span_imag.reshape(owner_shape))
    rounded = (span_real * ortho_scale).astype(jnp.bfloat16)
    returned = lax.all_to_all(rounded, "col", split_axis=1, concat_axis=4, tiled=True)
    layout = (row_count, fine_count, seq_count, row_count, sub_feats)
    spectrum = lax.all_to_all(
        returned.reshape(layout), "row", split_axis=0, concat_axis=4, tiled=True
    )
    spectrum = spectrum.reshape(fine_count, seq_count, row_count, feat_count)
    mixed = jnp.einsum("jskf,fd->sjkd", spectrum, w_out, preferred_element_type=jnp.float32).astype(
        jnp.bfloat16
    )
    return mixed.reshape(seq_count, fine_count * row_count, width)


def solution(mesh):
    return jax.shard_map(
        shards,
        mesh=mesh,
        in_specs=(P("grp", ("row", "col"), None), P(), P(), P()),
        out_specs=P("grp", ("row", "col"), None),
        check_vma=False,
    )
```

profile of v0, /device:TPU:6, one launch (start us, length us, event | category | flops | bytes accessed | tf_op | source)
XLA Modules:
  0.0 217.6 jit_solution(15632472128217325967)
XLA Ops:
  0.0 1.4 fusion.10
  1.4 0.7 convert_element_type.176
  2.1 2.3 %fusion.9 = bf16[512,128]{0,1:T(8,128)(2,1)S(1)} fusion(bf16[2048,512]{1,0:T(8,128)(2,1)} %param.6, bf16[1,128,2048]{2,1,0:T(8,128)(2,1)} %param.4, f32[2048]{0:T(1024)S(1)} %convert_element_type.176, f32[128]{0:T(128)S(1)} %add_rsqrt_fusion), kind=kOutput, calls=%fused_computation.20 | convolution fusion | flops 269549568 | bytes 2761216 | tf_op jit(solution)/shard_map/std,df->sft/dot_general | solution.py:61
  4.5 0.4 fusion.8
  4.9 0.4 convolution_convert_fusion.2
  5.7 1.3 pad_maximum_fusion
  7.0 83.1 %all-to-all-start = ((bf16[2,512,128]{2,0,1:T(2,128)(2,1)}), bf16[2,512,128]{2,0,1:T(2,128)(2,1)S(1)}, u32[]{:S(2)}, u32[]{:S(2)}) async-start(bf16[2,512,128]{2,0,1:T(2,128)(2,1)} %pad_maximum_fusion), calls=%async_computation | async-start | bytes 524288 | tf_op jit(solution)/shard_map/all_to_all | solution.py:18
  90.2 18.0 %all-to-all-done = bf16[2,512,128]{2,0,1:T(2,128)(2,1)S(1)} async-done(((bf16[2,512,128]{2,0,1:T(2,128)(2,1)}), bf16[2,512,128]{2,0,1:T(2,128)(2,1)S(1)}, u32[]{:S(2)}, u32[]{:S(2)}) %all-to-all-start) | async-done | bytes 262176 | tf_op jit(solution)/shard_map/all_to_all | solution.py:18
  108.8 0.2 fusion.6
  109.0 0.9 fusion.26
  109.9 31.5 %all_to_all.63 = bf16[16,32,1,128]{3,0,2,1:T(8,128)(2,1)S(1)} all-to-all(bf16[16,32,1,128]{3,0,2,1:T(8,128)(2,1)S(1)} %get-tuple-element.6), channel_id=1, replica_groups=mesh['grp'=2,'row'=16,'col'=32] {'col'}, dimensions={1} | all-to-all | bytes 262144 | tf_op jit(solution)/shard_map/all_to_all | solution.py:111
  141.4 4.8 %all-to-all-start.1 = ((bf16[16,32,1,128]{3,0,2,1:T(8,128)(2,1)}), bf16[16,32,1,128]{3,0,2,1:T(8,128)(2,1)S(1)}, u32[]{:S(2)}, u32[]{:S(2)}) async-start(bf16[16,32,1,128]{3,0,2,1:T(8,128)(2,1)} %get-tuple-element.5), calls=%async_computation.1 | async-start | bytes 262144 | tf_op jit(solution)/shard_map/all_to_all | solution.py:108
  146.3 0.2 fusion.28
  146.5 16.0 %all-to-all-done.1 = bf16[16,32,1,128]{3,0,2,1:T(8,128)(2,1)S(1)} async-done(((bf16[16,32,1,128]{3,0,2,1:T(8,128)(2,1)}), bf16[16,32,1,128]{3,0,2,1:T(8,128)(2,1)S(1)}, u32[]{:S(2)}, u32[]{:S(2)}) %all-to-all-start.1) | async-done | bytes 131104 | tf_op jit(solution)/shard_map/all_to_all | solution.py:108
  162.6 0.2 fusion.32
  162.8 0.3 fusion.4
  163.1 0.2 fusion.5
  163.3 0.6 fusion.18
  163.9 1.4 fusion.3
  165.3 1.8 copy.30
  167.1 1.3 copy.58
  168.4 2.5 %reshape.268 = bf16[32,2,1024]{2,1,0:T(2,128)(2,1)S(1)} reshape(bf16[32,1,16,8,16]{4,3,2,1,0:T(8,128)(2,1)} %bitcast.142) | data formatting | bytes 262144
  170.9 20.3 %all_to_all.64 = bf16[32,2,1024]{2,1,0:T(2,128)(2,1)S(1)} all-to-all(bf16[32,2,1024]{2,1,0:T(2,128)(2,1)S(1)} %reshape.268), channel_id=1, replica_groups=mesh['grp'=2,'row'=16,'col'=32] {'col'}, dimensions={0} | all-to-all | bytes 262144 | tf_op jit(solution)/shard_map/all_to_all | solution.py:120
  191.2 0.7 reshape.269
  191.9 1.0 bitcast_bitcast_fusion
  192.9 2.2 %copy.32 = bf16[16,8,1,16,32]{4,3,2,1,0:T(8,128)(2,1)S(1)} copy(bf16[16,8,1,16,32]{3,1,0,4,2:T(8,128)(2,1)} %bitcast_bitcast_fusion) | data formatting | bytes 262144 | tf_op jit(solution)/shard_map/reshape | solution.py:123
  195.1 0.5 reshape.270
  195.7 19.6 %all_to_all.65 = bf16[16,2,2048]{2,1,0:T(2,128)(2,1)S(1)} all-to-all(bf16[16,2,2048]{2,1,0:T(2,128)(2,1)S(1)} %reshape.270), channel_id=1, replica_groups=mesh['grp'=2,'row'=16,'col'=32] {'row'}, dimensions={0} | all-to-all | bytes 262144 | tf_op jit(solution)/shard_map/all_to_all | solution.py:122
  215.3 0.3 reshape.271
  215.6 0.3 copy.33
  215.9 0.4 reshape.255
  216.4 1.2 convolution_convert_fusion
  (13 shorter events, 1.3 us)
Async XLA Ops:
  0.0 216.4 %copy-start = (bf16[512,2048]{1,0:T(8,128)(2,1)S(1)}, bf16[512,2048]{1,0:T(8,128)(2,1)}, u32[]{:S(2)}) copy-start(bf16[512,2048]{1,0:T(8,128)(2,1)} %param.7) | copy-start | bytes 6291460
  7.0 101.2 %all-to-all-start = ((bf16[2,512,128]{2,0,1:T(2,128)(2,1)}), bf16[2,512,128]{2,0,1:T(2,128)(2,1)S(1)}, u32[]{:S(2)}, u32[]{:S(2)}) async-start(bf16[2,512,128]{2,0,1:T(2,128)(2,1)} %pad_maximum_fusion), calls=%async_computation | async-start | bytes 524288 | tf_op jit(solution)/shard_map/all_to_all | solution.py:18
  141.4 21.2 %all-to-all-start.1 = ((bf16[16,32,1,128]{3,0,2,1:T(8,128)(2,1)}), bf16[16,32,1,128]{3,0,2,1:T(8,128)(2,1)S(1)}, u32[]{:S(2)}, u32[]{:S(2)}) async-start(bf16[16,32,1,128]{3,0,2,1:T(8,128)(2,1)} %get-tuple-element.5), calls=%async_computation.1 | async-start | bytes 262144 | tf_op jit(solution)/shard_map/all_to_all | solution.py:108
where the time goes:
time: 218 us
  starting transfers between devices  87.9 us (40%)
  blocking collectives  71.4 us (33%)
  waiting for transfers between devices  34.1 us (16%)
  local copies, waits for them, and re-layouts  11.8 us (5%)
  matrix products  8.81 us (4%)
  other arithmetic  3.54 us (2%)
    all_to_all x1, starting transfers between devices, side_by_side(): lax.all_to_all(both, axis, split_axis=split_dim, concat_axis=concat_dim,...  83.1 us
    all_to_all x1, blocking collectives, shards(): lax.all_to_all(sending[1].astype(jnp.bfloat16), 'col', split_axis=1, conc...  31.5 us
    all_to_all x1, blocking collectives, shards(): lax.all_to_all(rounded, 'col', split_axis=1, concat_axis=4, tiled=True)  20.3 us
    all_to_all x1, blocking collectives, shards(): lax.all_to_all(returned.reshape(layout), 'row', split_axis=0, concat_axis...  19.6 us
    all_to_all x1, waiting for transfers between devices, side_by_side(): lax.all_to_all(both, axis, split_axis=split_dim, concat_axis=concat_dim,...  18 us
    all_to_all x1, waiting for transfers between devices, shards(): lax.all_to_all(sending[0].astype(jnp.bfloat16), 'col', split_axis=1, conc...  16 us
    all_to_all x1, starting transfers between devices, shards(): lax.all_to_all(sending[0].astype(jnp.bfloat16), 'col', split_axis=1, conc...  4.78 us
    dot_general x10, matrix products, apply(): return jnp.einsum(pattern, table, data)  4.53 us
  transfers between devices with their start and end apart: 2, of which 2 were waited for; matrix products, arithmetic and copies ran while one was open for 0% of the time, Pallas kernels for 0%

commit v1 on v0

v1 whole, which is shorter than its diff:
```python
import functools
import math

import jax
import jax.numpy as jnp
import numpy as np
from jax import lax
from jax.experimental import pallas as pl
from jax.experimental.pallas import tpu as pltpu
from jax.sharding import PartitionSpec as P

GROUP_CH = 128
NORM_EPS = 1e-06
CHUNKS = 4
VMEM_LIMIT = 16 * 1024 * 1024

BF16 = jnp.bfloat16
F32 = jnp.float32


def channel_tables():
    half = GROUP_CH // 2
    q = np.arange(GROUP_CH)[:, None]
    f = np.arange(GROUP_CH)[None, :]
    freq = np.where(f <= half, f, GROUP_CH - f)
    angle = 2.0 * np.pi * (q * freq % GROUP_CH) / GROUP_CH
    spread = np.where(f <= half, np.cos(angle), np.sin(angle))
    merge = np.zeros((GROUP_CH, GROUP_CH))
    merge[0, 0] = merge[half, half] = 1.0
    for m in range(1, half):
        merge[m, m] = merge[m, GROUP_CH - m] = 1.0
        merge[GROUP_CH - m, m] = -1.0
        merge[GROUP_CH - m, GROUP_CH - m] = 1.0
    return spread, merge


def sequence_tables(rows, cols, toks):
    length = rows * cols * toks
    low = 2 * toks
    high = length // low
    assert high == low
    halves = cols // 2
    a = (np.arange(rows)[None, :] * halves + np.arange(halves)[:, None]).reshape(-1)
    k1 = np.arange(high)
    first = 2.0 * np.pi * (a[:, None] * k1[None, :] % high) / high
    b = np.arange(low)
    turn = 2.0 * np.pi * (b[:, None] * k1[None, :] % length) / length
    last = 2.0 * np.pi * (a[:, None] * b[None, :] % low) / low
    scale = 1.0 / math.sqrt(length * GROUP_CH)
    return (
        np.concatenate([np.cos(first), -np.sin(first)], axis=1),
        np.stack([np.cos(turn) * scale, -np.sin(turn) * scale]),
        np.concatenate([np.cos(last), np.sin(last)], axis=1),
    )


def project(tok_hbm, gain_ref, w_hbm, spread_ref, out_ref, tok_v, w_v, sems):
    toks, width = tok_v.shape
    part = width // CHUNKS
    copies = []
    for j in range(CHUNKS):
        at = pl.ds(j * part, part)
        copies.append(
            (
                pltpu.make_async_copy(tok_hbm.at[0, :, at], tok_v.at[:, at], sems.at[0, j]),
                pltpu.make_async_copy(w_hbm.at[at, :], w_v.at[at, :], sems.at[1, j]),
            )
        )
    for pair in copies:
        for copy in pair:
            copy.start()
    squares = jnp.zeros((toks, 1), F32)
    total = jnp.zeros((toks, w_v.shape[1]), F32)
    for j in range(CHUNKS):
        at = pl.ds(j * part, part)
        copies[j][0].wait()
        x = tok_v[:, at].astype(F32)
        squares += jnp.sum(x * x, axis=-1, keepdims=True)
        scaled = (x * gain_ref[:, at].astype(F32)).astype(BF16)
        copies[j][1].wait()
        total += jnp.dot(scaled, w_v[at, :], preferred_element_type=F32)
    factor = lax.rsqrt(squares * (1.0 / width) + NORM_EPS)
    mixin = (total * factor).astype(BF16)
    for g in range(w_v.shape[1] // GROUP_CH):
        at = slice(g * GROUP_CH, (g + 1) * GROUP_CH)
        out_ref[at, :] = lax.dot_general(
            spread_ref[...], mixin[:, at], (((0,), (1,)), ((), ())), preferred_element_type=F32
        ).astype(BF16)


def transform(which_ref, x_ref, first_ref, turn_ref, last_ref, out_ref):
    halves, _, rows, toks = x_ref.shape
    high = first_ref.shape[0]
    sine = which_ref[0] == 1
    parts = []
    for c in range(2):
        x = x_ref[:, c].reshape(halves * rows, toks)
        parts.append(
            lax.dot_general(x, first_ref[...], (((0,), (0,)), ((), ())), preferred_element_type=F32)
        )
    y = jnp.concatenate(parts, axis=0)
    y_re, y_im = y[:, :high], y[:, high:]
    w_re, w_im = turn_ref[0], turn_ref[1]
    u_re = y_re * w_re - y_im * w_im
    u_im = y_re * w_im + y_im * w_re
    both = jnp.concatenate(
        [jnp.where(sine, -u_im, u_re).astype(BF16), jnp.where(sine, u_re, u_im).astype(BF16)],
        axis=0,
    )
    z = jnp.dot(last_ref[...], both, preferred_element_type=F32).astype(BF16)
    for c in range(2):
        out_ref[:, c] = z[:, c * toks : (c + 1) * toks].reshape(halves, rows, toks)


def merge_out(x_ref, merge_ref, w_ref, out_ref):
    feats = x_ref.shape[0]
    pieces = []
    for g in range(feats // GROUP_CH):
        at = slice(g * GROUP_CH, (g + 1) * GROUP_CH)
        pieces.append(
            lax.dot_general(
                x_ref[at, :], merge_ref[...], (((0,), (0,)), ((), ())), preferred_element_type=F32
            ).astype(BF16)
        )
    spectrum = jnp.concatenate(pieces, axis=1)
    out_ref[0] = jnp.dot(spectrum, w_ref[...], preferred_element_type=F32).astype(BF16)


def shards(rows, cols, tokens, norm_gain, w_in, w_out):
    _, toks, width = tokens.shape
    feats = w_in.shape[1]
    halves = cols // 2
    spread, merge = channel_tables()
    first, turn, last = sequence_tables(rows, cols, toks)
    vmem = pl.BlockSpec(memory_space=pltpu.VMEM)
    smem = pl.BlockSpec(memory_space=pltpu.SMEM)
    hbm = pl.BlockSpec(memory_space=pl.ANY)

    feature = lax.axis_index("row") * cols + lax.axis_index("col")
    sine = (feature % GROUP_CH > GROUP_CH // 2).astype(jnp.int32).reshape(1)

    sent = pl.pallas_call(
        project,
        out_shape=jax.ShapeDtypeStruct((feats, toks), BF16),
        in_specs=[hbm, vmem, hbm, vmem],
        out_specs=vmem,
        scratch_shapes=[
            pltpu.VMEM((toks, width), BF16),
            pltpu.VMEM((width, feats), BF16),
            pltpu.SemaphoreType.DMA((2, CHUNKS)),
        ],
        name="project",
    )(tokens, norm_gain.reshape(1, width), w_in, jnp.asarray(spread, BF16))
    sent = lax.all_to_all(
        sent.reshape(rows, cols, toks), "row", split_axis=0, concat_axis=0, tiled=True
    )
    sent = lax.all_to_all(
        sent.transpose(1, 0, 2), "col", split_axis=0, concat_axis=0, tiled=True
    )
    back = pl.pallas_call(
        transform,
        out_shape=jax.ShapeDtypeStruct((halves, 2, rows, toks), BF16),
        in_specs=[smem, vmem, vmem, vmem, vmem],
        out_specs=vmem,
        compiler_params=pltpu.CompilerParams(vmem_limit_bytes=VMEM_LIMIT),
        name="transform",
    )(
        sine,
        sent.reshape(halves, 2, rows, toks),
        jnp.asarray(first, BF16),
        jnp.asarray(turn, F32),
        jnp.asarray(last, BF16),
    )
    back = lax.all_to_all(
        back.reshape(cols, rows, toks), "col", split_axis=0, concat_axis=0, tiled=True
    )
    back = lax.all_to_all(
        back.transpose(1, 0, 2), "row", split_axis=0, concat_axis=0, tiled=True
    )
    return pl.pallas_call(
        merge_out,
        out_shape=jax.ShapeDtypeStruct((1, toks, width), BF16),
        in_specs=[vmem, vmem, vmem],
        out_specs=vmem,
        compiler_params=pltpu.CompilerParams(vmem_limit_bytes=VMEM_LIMIT),
        name="merge_out",
    )(back.reshape(feats, toks), jnp.asarray(merge, BF16), w_out)


def solution(mesh):
    return jax.shard_map(
        functools.partial(shards, mesh.shape["row"], mesh.shape["col"]),
        mesh=mesh,
        in_specs=(P("grp", ("row", "col"), None), P(), P(), P()),
        out_specs=P("grp", ("row", "col"), None),
        check_vma=False,
    )
```

time: 218 us -> 176 us (0.81)
  starting transfers between devices: 87.9 us -> 15.2 us
  blocking collectives: 71.4 us -> 136 us
  waiting for transfers between devices: 34.1 us -> 16.5 us
  local copies, waits for them, and re-layouts: 11.8 us -> 2.15 us
  matrix products: 8.81 us -> 0 us
  Pallas kernels: 0 us -> 5.64 us
  other arithmetic: 3.54 us -> 0 us
    all_to_all x2 -> x1, starting transfers between devices: 87.9 us -> 15.2 us  [shards(): lax.all_to_all(sent.transpose(1, 0, 2), 'col', split_axis=0, concat_axis=...]
    all_to_all x3, blocking collectives: 71.4 us -> 136 us  [the longest x1 97.9 us: shards(): lax.all_to_all(sent.reshape(rows, cols, toks), 'row', split_axis=0, conca...]
    all_to_all x2 -> x1, waiting for transfers between devices: 34.1 us -> 16.5 us  [shards(): lax.all_to_all(sent.transpose(1, 0, 2), 'col', split_axis=0, concat_axis=...]
    dot_general x14 -> x0, matrix products: 8.81 us -> none  [the longest x10 4.53 us: apply(): return jnp.einsum(pattern, table, data)]
    pallas_call x0 -> x3, Pallas kernels: none -> 5.64 us  [the longest x1 3.77 us: shards(): pl.pallas_call(project, out_shape=jax.ShapeDtypeStruct((feats, toks), BF1...]
    unnamed x6 -> x10, local copies, waits for them, and re-layouts: 3.99 us -> 0.02 us
    convert_element_type x4 -> x0, local copies, waits for them, and re-layouts: 3.47 us -> none  [the longest x2 3.06 us: shards(): rounded = (span_real * ortho_scale).astype(jnp.bfloat16)]
  transfers between devices with their start and end apart: 2 -> 1, of which waited for: 2 -> 1; matrix products, arithmetic and copies ran while one was open for 0% -> 0% of each run, Pallas kernels for 0% -> 0%
where the time goes in v1:
time: 176 us; the launch traced here: 175 us
  blocking collectives  136 us (77%)
  waiting for transfers between devices  16.5 us (9%)
  starting transfers between devices  15.2 us (9%)
  Pallas kernels  5.64 us (3%)
  local copies, waits for them, and re-layouts  2.15 us (1%)
    all_to_all x1, blocking collectives, shards(): lax.all_to_all(sent.reshape(rows, cols, toks), 'row', split_axis=0, conca...  97.9 us
    all_to_all x1, blocking collectives, shards(): lax.all_to_all(back.reshape(cols, rows, toks), 'col', split_axis=0, conca...  20.3 us
    all_to_all x1, blocking collectives, shards(): lax.all_to_all(back.transpose(1, 0, 2), 'row', split_axis=0, concat_axis=...  17.6 us
    all_to_all x1, waiting for transfers between devices, shards(): lax.all_to_all(sent.transpose(1, 0, 2), 'col', split_axis=0, concat_axis=...  16.5 us
    all_to_all x1, starting transfers between devices, shards(): lax.all_to_all(sent.transpose(1, 0, 2), 'col', split_axis=0, concat_axis=...  15.2 us
    pallas_call x1, Pallas kernels, shards(): pl.pallas_call(project, out_shape=jax.ShapeDtypeStruct((feats, toks), BF1...  3.77 us
  transfers between devices with their start and end apart: 1, of which 1 were waited for; matrix products, arithmetic and copies ran while one was open for 0% of the time, Pallas kernels for 0%

profile of v1, /device:TPU:6, one launch (start us, length us, event | category | flops | bytes accessed | tf_op | source)
XLA Modules:
  0.0 175.2 jit_solution(6025922651845650471)
XLA Ops:
  0.0 0.0 copy-start.2
  0.0 0.0 copy-start.1
  0.0 0.0 copy-start.3
  0.0 1.4 reshape.22.gain_ref
  1.4 3.8 %project.1 = bf16[512,128]{1,0:T(8,128)(2,1)} custom-call(bf16[1,128,2048]{2,1,0:T(8,128)(2,1)} %tok_hbm.1, bf16[1,2048]{1,0:T(2,128)(2,1)} %reshape.22.gain_ref, bf16[2048,512]{1,0:T(8,128)(2,1)} %w_hbm.1, bf16[128,128]{1,0:T(8,128)(2,1)} %constant.36.clone.spread_ref), custom_call_target="tpu_custom_call" | custom-call | tf_op jit(solution)/shard_map/project/pallas_call | solution.py:142
  5.2 0.0 copy-start
  5.2 0.0 copy-start.4
  5.2 97.9 %all_to_all.20 = bf16[16,32,128]{2,1,0:T(8,128)(2,1)S(1)} all-to-all(bf16[16,32,128]{2,1,0:T(8,128)(2,1)} %bitcast.10), channel_id=1, replica_groups=mesh['grp'=2,'row'=16,'col'=32] {'row'}, dimensions={0} | all-to-all | bytes 262144 | tf_op jit(solution)/shard_map/all_to_all | solution.py:154
  103.1 0.7 copy.14
  103.8 15.2 %all-to-all-start.1 = ((bf16[32,16,128]{2,1,0:T(8,128)(2,1)}), bf16[32,16,128]{2,1,0:T(8,128)(2,1)S(1)}, u32[]{:S(2)}, u32[]{:S(2)}) async-start(bf16[32,16,128]{2,1,0:T(8,128)(2,1)} %copy.14), calls=%async_computation.1 | async-start | bytes 262144 | tf_op jit(solution)/shard_map/all_to_all | solution.py:157
  119.0 16.5 %all-to-all-done.1 = bf16[32,16,128]{2,1,0:T(8,128)(2,1)S(1)} async-done(((bf16[32,16,128]{2,1,0:T(8,128)(2,1)}), bf16[32,16,128]{2,1,0:T(8,128)(2,1)S(1)}, u32[]{:S(2)}, u32[]{:S(2)}) %all-to-all-start.1) | async-done | bytes 131104 | tf_op jit(solution)/shard_map/all_to_all | solution.py:157
  135.4 0.0 copy-done.2
  135.4 0.0 copy-done.1
  135.4 0.0 copy-done.3
  135.4 0.5 transform.1
  135.9 20.3 %all_to_all.21 = bf16[32,16,128]{2,1,0:T(8,128)(2,1)S(1)} all-to-all(bf16[32,16,128]{2,1,0:T(8,128)(2,1)S(1)} %bitcast.8), channel_id=1, replica_groups=mesh['grp'=2,'row'=16,'col'=32] {'col'}, dimensions={0} | all-to-all | bytes 262144 | tf_op jit(solution)/shard_map/all_to_all | solution.py:174
  156.2 17.6 %all_to_all.22 = bf16[16,32,128]{2,1,0:T(8,128)(2,1)S(1)} all-to-all(bf16[16,32,128]{2,1,0:T(8,128)(2,1)S(1)} %copy.15), channel_id=1, replica_groups=mesh['grp'=2,'row'=16,'col'=32] {'row'}, dimensions={0} | all-to-all | bytes 262144 | tf_op jit(solution)/shard_map/all_to_all | solution.py:177
  173.8 0.0 copy-done
  173.8 0.0 copy-done.4
  173.8 1.4 merge_out.1
  (1 shorter events, 0.0 us)
Async XLA Ops:
  0.0 135.4 %copy-start.2 = (bf16[256,512]{1,0:T(8,128)(2,1)S(1)}, bf16[256,512]{1,0:T(8,128)(2,1)}, u32[]{:S(2)}) copy-start(bf16[256,512]{1,0:T(8,128)(2,1)} %constant.39.clone.last_ref) | copy-start | bytes 786436
  0.0 135.4 %copy-start.1 = (f32[2,256,256]{2,1,0:T(8,128)S(1)}, f32[2,256,256]{2,1,0:T(8,128)}, u32[]{:S(2)}) copy-start(f32[2,256,256]{2,1,0:T(8,128)} %constant.38.clone.turn_ref) | copy-start | bytes 1572868
  0.0 135.4 %copy-start.3 = (bf16[256,512]{1,0:T(8,128)(2,1)S(1)}, bf16[256,512]{1,0:T(8,128)(2,1)}, u32[]{:S(2)}) copy-start(bf16[256,512]{1,0:T(8,128)(2,1)} %constant.37.clone.first_ref) | copy-start | bytes 786436
  5.2 168.6 %copy-start = (bf16[512,2048]{1,0:T(8,128)(2,1)S(1)}, bf16[512,2048]{1,0:T(8,128)(2,1)}, u32[]{:S(2)}) copy-start(bf16[512,2048]{1,0:T(8,128)(2,1)} %w_ref.1) | copy-start | bytes 6291460
  5.2 168.6 %copy-start.4 = (bf16[128,128]{1,0:T(8,128)(2,1)S(1)}, bf16[128,128]{1,0:T(8,128)(2,1)}, u32[]{:S(2)}) copy-start(bf16[128,128]{1,0:T(8,128)(2,1)} %constant.40.clone.merge_ref) | copy-start | bytes 98308
  103.8 31.7 %all-to-all-start.1 = ((bf16[32,16,128]{2,1,0:T(8,128)(2,1)}), bf16[32,16,128]{2,1,0:T(8,128)(2,1)S(1)}, u32[]{:S(2)}, u32[]{:S(2)}) async-start(bf16[32,16,128]{2,1,0:T(8,128)(2,1)} %copy.14), calls=%async_computation.1 | async-start | bytes 262144 | tf_op jit(solution)/shard_map/all_to_all | solution.py:157

commit v2 on v1

v2 whole, which is shorter than its diff:
```python
import functools
import math

import jax
import jax.numpy as jnp
import numpy as np
from jax import lax
from jax.experimental import pallas as pl
from jax.experimental.pallas import tpu as pltpu
from jax.sharding import PartitionSpec as P

GROUP_CH = 128
NORM_EPS = 1e-06
CORES = 2
CHUNKS = 4
VMEM_LIMIT = 16 * 1024 * 1024
PROJECT_LIMIT = 60 * 1024 * 1024

BF16 = jnp.bfloat16
F32 = jnp.float32


def channel_tables():
    half = GROUP_CH // 2
    q = np.arange(GROUP_CH)[:, None]
    f = np.arange(GROUP_CH)[None, :]
    freq = np.where(f <= half, f, GROUP_CH - f)
    angle = 2.0 * np.pi * (q * freq % GROUP_CH) / GROUP_CH
    spread = np.where(f <= half, np.cos(angle), np.sin(angle))
    merge = np.zeros((GROUP_CH, GROUP_CH))
    merge[0, 0] = merge[half, half] = 1.0
    for m in range(1, half):
        merge[m, m] = merge[m, GROUP_CH - m] = 1.0
        merge[GROUP_CH - m, m] = -1.0
        merge[GROUP_CH - m, GROUP_CH - m] = 1.0
    return spread, merge


def sequence_tables(rows, chips, toks):
    length = rows * chips * CORES * toks
    low = CORES * toks
    high = rows * chips
    assert high == low
    a = (np.arange(rows)[None, :] * chips + np.arange(chips)[:, None]).reshape(-1)
    k1 = np.arange(high)
    b = np.arange(low)
    first = 2.0 * np.pi * (a[:, None] * k1[None, :] % high) / high
    turn = 2.0 * np.pi * (b[:, None] * k1[None, :] % length) / length
    last = 2.0 * np.pi * (a[:, None] * b[None, :] % low) / low
    scale = 1.0 / math.sqrt(length * GROUP_CH)

    def halves(table):
        return [table[..., h * toks : (h + 1) * toks] for h in range(CORES)]

    first = np.stack([np.concatenate([np.cos(t), -np.sin(t)], axis=1) for t in halves(first)])
    turn = np.stack(
        [
            np.stack([np.stack([np.cos(t), -np.sin(t)]) * scale for t in halves(turn[c * toks : (c + 1) * toks])])
            for c in range(CORES)
        ]
    )
    last = np.stack([np.concatenate([np.cos(t), np.sin(t)], axis=1) for t in halves(last)])
    return first, turn, last


def project(tok_hbm, gain_hbm, w_hbm, spread_hbm, out_ref, tok_v, w_v, gain_v, spread_v, sems, small_sems):
    toks, width = tok_v.shape
    part = width // CHUNKS
    small = [
        pltpu.make_async_copy(gain_hbm, gain_v, small_sems.at[0]),
        pltpu.make_async_copy(spread_hbm, spread_v, small_sems.at[1]),
    ]
    copies = []
    for j in range(CHUNKS):
        at = pl.ds(j * part, part)
        copies.append(
            (
                pltpu.make_async_copy(tok_hbm.at[0, :, at], tok_v.at[:, at], sems.at[0, j]),
                pltpu.make_async_copy(w_hbm.at[at, :], w_v.at[at, :], sems.at[1, j]),
            )
        )
    small[0].start()
    for pair in copies:
        for copy in pair:
            copy.start()
    small[1].start()
    small[0].wait()
    gain = gain_v[...].astype(F32).reshape(1, width)
    squares = jnp.zeros((toks, 1), F32)
    total = jnp.zeros((toks, w_v.shape[1]), F32)
    for j in range(CHUNKS):
        at = slice(j * part, (j + 1) * part)
        copies[j][0].wait()
        x = tok_v[:, at].astype(F32)
        squares += jnp.sum(x * x, axis=-1, keepdims=True)
        scaled = (x * gain[:, at]).astype(BF16)
        copies[j][1].wait()
        total += jnp.dot(scaled, w_v[at, :], preferred_element_type=F32)
    factor = lax.rsqrt(squares * (1.0 / width) + NORM_EPS)
    mixin = (total * factor).astype(BF16)
    small[1].wait()
    for g in range(w_v.shape[1] // GROUP_CH):
        at = slice(g * GROUP_CH, (g + 1) * GROUP_CH)
        out_ref[at, :] = lax.dot_general(
            spread_v[...], mixin[:, at], (((0,), (1,)), ((), ())), preferred_element_type=F32
        ).astype(BF16)


def transform_a(which_ref, x_ref, first_ref, turn_ref, own_ref, send_ref):
    chips, _, rows, toks = x_ref.shape
    core = which_ref[0]
    for half, ref in ((core, own_ref), (1 - core, send_ref)):
        table = first_ref[half]
        w_re, w_im = turn_ref[core, half, 0], turn_ref[core, half, 1]
        for j in range(CORES):
            sine = which_ref[1 + j] == 1
            y = lax.dot_general(
                x_ref[:, j].reshape(chips * rows, toks),
                table,
                (((0,), (0,)), ((), ())),
                preferred_element_type=F32,
            )
            y_re, y_im = y[:, :toks], y[:, toks:]
            u_re = (y_re * w_re - y_im * w_im).astype(BF16)
            u_im = (y_re * w_im + y_im * w_re).astype(BF16)
            at = slice(j * toks, (j + 1) * toks)
            ref[:toks, at] = jnp.where(sine, -u_im, u_re)
            ref[toks:, at] = jnp.where(sine, u_re, u_im)


def transform_b(which_ref, own_ref, got_ref, last_ref, out_ref):
    chips, _, rows, toks = out_ref.shape
    core = which_ref[0]
    z = jnp.dot(last_ref[core], own_ref[...], preferred_element_type=F32)
    z += jnp.dot(last_ref[1 - core], got_ref[...], preferred_element_type=F32)
    z = z.astype(BF16)
    for j in range(CORES):
        out_ref[:, j] = z[:, j * toks : (j + 1) * toks].reshape(chips, rows, toks)


def merge_out(x_ref, merge_ref, w_ref, out_hbm, out_v, sems):
    feats = x_ref.shape[0]
    width = w_ref.shape[1]
    pieces = []
    for g in range(feats // GROUP_CH):
        at = slice(g * GROUP_CH, (g + 1) * GROUP_CH)
        pieces.append(
            lax.dot_general(
                x_ref[at, :], merge_ref[...], (((0,), (0,)), ((), ())), preferred_element_type=F32
            ).astype(BF16)
        )
    spectrum = jnp.concatenate(pieces, axis=1)
    part = width // CHUNKS
    copies = []
    for j in range(CHUNKS):
        at = slice(j * part, (j + 1) * part)
        out_v[:, at] = jnp.dot(spectrum, w_ref[:, at], preferred_element_type=F32).astype(BF16)
        copies.append(
            pltpu.make_async_copy(
                out_v.at[:, pl.ds(j * part, part)],
                out_hbm.at[0, :, pl.ds(j * part, part)],
                sems.at[j],
            )
        )
        copies[-1].start()
    for copy in copies:
        copy.wait()


VMEM = pl.BlockSpec(memory_space=pltpu.VMEM)
SMEM = pl.BlockSpec(memory_space=pltpu.SMEM)
HBM = pl.BlockSpec(memory_space=pltpu.HBM)


def call_project(tokens, norm_gain, w_in, spread):
    _, toks, width = tokens.shape
    feats = w_in.shape[1]
    return pl.pallas_call(
        project,
        out_shape=jax.ShapeDtypeStruct((feats, toks), BF16),
        in_specs=[HBM, HBM, HBM, HBM],
        out_specs=VMEM,
        scratch_shapes=[
            pltpu.VMEM((toks, width), BF16),
            pltpu.VMEM((width, feats), BF16),
            pltpu.VMEM(norm_gain.shape, BF16),
            pltpu.VMEM(spread.shape, BF16),
            pltpu.SemaphoreType.DMA((2, CHUNKS)),
            pltpu.SemaphoreType.DMA((2,)),
        ],
        compiler_params=pltpu.CompilerParams(vmem_limit_bytes=PROJECT_LIMIT),
        name="project",
    )(tokens, norm_gain, w_in, spread)


def call_transform_a(which, x, first, turn):
    toks = x.shape[-1]
    half = jax.ShapeDtypeStruct((2 * toks, CORES * toks), BF16)
    return pl.pallas_call(
        transform_a,
        out_shape=(half, half),
        in_specs=[SMEM, VMEM, VMEM, VMEM],
        out_specs=(VMEM, VMEM),
        compiler_params=pltpu.CompilerParams(vmem_limit_bytes=VMEM_LIMIT),
        name="transform_a",
    )(which, x, first, turn)


def call_transform_b(which, own, got, last, shape):
    return pl.pallas_call(
        transform_b,
        out_shape=jax.ShapeDtypeStruct(shape, BF16),
        in_specs=[SMEM, VMEM, VMEM, VMEM],
        out_specs=VMEM,
        compiler_params=pltpu.CompilerParams(vmem_limit_bytes=VMEM_LIMIT),
        name="transform_b",
    )(which, own, got, last)


def call_merge_out(x, merge, w_out):
    width = w_out.shape[1]
    toks = x.shape[1]
    return pl.pallas_call(
        merge_out,
        out_shape=jax.ShapeDtypeStruct((1, toks, width), BF16),
        in_specs=[VMEM, VMEM, VMEM],
        out_specs=HBM,
        scratch_shapes=[pltpu.VMEM((toks, width), BF16), pltpu.SemaphoreType.DMA((CHUNKS,))],
        compiler_params=pltpu.CompilerParams(vmem_limit_bytes=VMEM_LIMIT),
        name="merge_out",
    )(x, merge, w_out)


def shards(rows, cols, tokens, norm_gain, w_in, w_out):
    _, toks, width = tokens.shape
    feats = w_in.shape[1]
    chips = cols // CORES
    spread, merge = channel_tables()
    first, turn, last = sequence_tables(rows, chips, toks)
    lines = [[CORES * y + c for y in range(chips)] for c in range(CORES)]
    pairs = [(i, i ^ 1) for i in range(cols)]

    col = lax.axis_index("col")
    core = col % CORES
    feature = lax.axis_index("row") * cols + (col - core)
    which = jnp.stack(
        [core] + [((feature + j) % GROUP_CH > GROUP_CH // 2).astype(jnp.int32) for j in range(CORES)]
    )
    which, tokens = lax.optimization_barrier((which, tokens))

    def along_row(x):
        return lax.all_to_all(x, "row", split_axis=0, concat_axis=0, tiled=True)

    def along_line(x):
        return lax.all_to_all(
            x, "col", split_axis=0, concat_axis=0, tiled=True, axis_index_groups=lines
        )

    sent = call_project(tokens, norm_gain, w_in, jnp.asarray(spread, BF16))
    sent = along_row(sent.reshape(rows, cols, toks))
    sent = along_line(sent.transpose(1, 0, 2))
    shape = (chips, CORES, rows, toks)
    own, give = call_transform_a(
        which, sent.reshape(shape), jnp.asarray(first, BF16), jnp.asarray(turn, F32)
    )
    got = lax.ppermute(give, "col", pairs)
    back = call_transform_b(which, own, got, jnp.asarray(last, BF16), shape)
    back = along_line(back.reshape(cols, rows, toks))
    back = along_row(back.transpose(1, 0, 2))
    return call_merge_out(back.reshape(feats, toks), jnp.asarray(merge, BF16), w_out)


def solution(mesh):
    return jax.shard_map(
        functools.partial(shards, mesh.shape["row"], mesh.shape["col"]),
        mesh=mesh,
        in_specs=(P("grp", ("row", "col"), None), P(), P(), P()),
        out_specs=P("grp", ("row", "col"), None),
        check_vma=False,
    )
```

time: 176 us -> 172 us (0.977)
  blocking collectives: 136 us -> 161 us
  waiting for transfers between devices: 16.5 us -> 1.31 us
  starting transfers between devices: 15.2 us -> 1.95 us
  local copies, waits for them, and re-layouts: 2.15 us -> 0.11 us
    all_to_all x3 -> x4, blocking collectives: 136 us -> 161 us  [the longest x2 115 us: along_row(): return lax.all_to_all(x, 'row', split_axis=0, concat_axis=0, tiled=True)]
    all_to_all x1 -> x0, waiting for transfers between devices: 16.5 us -> none  [shards(): lax.all_to_all(sent.transpose(1, 0, 2), 'col', split_axis=0, concat_axis=...]
    all_to_all x1 -> x0, starting transfers between devices: 15.2 us -> none  [shards(): lax.all_to_all(sent.transpose(1, 0, 2), 'col', split_axis=0, concat_axis=...]
    ppermute x0 -> x1, starting transfers between devices: none -> 1.95 us  [shards(): got = lax.ppermute(give, 'col', pairs)]
    pallas_call x3 -> x4, Pallas kernels: 5.64 us -> 6.31 us  [the longest x1 3.41 us: call_project(): pl.pallas_call(project, out_shape=jax.ShapeDtypeStruct((feats, toks), BF1...]
where the time goes in v2:
time: 172 us; the launch traced here: 171 us
  blocking collectives  161 us (94%)
  Pallas kernels  6.31 us (4%)
  starting transfers between devices  1.95 us (1%)
    all_to_all x2, blocking collectives, along_row(): return lax.all_to_all(x, 'row', split_axis=0, concat_axis=0, tiled=True)  115 us
    all_to_all x2, blocking collectives, along_line(): lax.all_to_all(x, 'col', split_axis=0, concat_axis=0, tiled=True, axis_in...  45.7 us
  transfers between devices with their start and end apart: 1, of which 1 were waited for; matrix products, arithmetic and copies ran while one was open for 0% of the time, Pallas kernels for 0%

profile of v2, /device:TPU:6, one launch (start us, length us, event | category | flops | bytes accessed | tf_op | source)
XLA Modules:
  0.0 171.0 jit_solution(12689867146928136498)
XLA Ops:
  0.0 0.0 copy-start.1
  0.0 0.0 copy-start.2
  0.0 0.1 pad_add_fusion.which_ref
  0.1 0.0 copy-start.3
  0.1 3.4 %project.1 = bf16[512,128]{1,0:T(8,128)(2,1)} custom-call(bf16[1,128,2048]{2,1,0:T(8,128)(2,1)} %tok_hbm, bf16[2048]{0:T(1024)(128)(2,1)} %gain_hbm.1, bf16[2048,512]{1,0:T(8,128)(2,1)} %w_hbm.1, bf16[128,128]{1,0:T(8,128)(2,1)} %constant.51.clone.spread_hbm), custom_call_target="tpu_custom_call" | custom-call | tf_op jit(solution)/shard_map/project/pallas_call | solution.py:178
  3.5 0.0 copy-start
  3.5 0.0 copy-start.4
  3.5 97.9 %all_to_all.20 = bf16[16,32,128]{2,1,0:T(8,128)(2,1)S(1)} all-to-all(bf16[16,32,128]{2,1,0:T(8,128)(2,1)} %bitcast.12), channel_id=1, replica_groups=mesh['grp'=2,'row'=16,'col'=32] {'row'}, dimensions={0} | all-to-all | bytes 262144 | tf_op jit(solution)/shard_map/all_to_all | solution.py:252
  101.4 0.1 copy.14
  101.4 27.1 %all_to_all.21 = bf16[32,16,128]{2,1,0:T(8,128)(2,1)S(1)} all-to-all(bf16[32,16,128]{2,1,0:T(8,128)(2,1)S(1)} %copy.14), channel_id=1, replica_groups={{0,2,4,6,8,10,12,14,16,18,20,22,24,26,28,30},{1,3,5,7,9,11,13,15,17,19,..., dimensions={0} | all-to-all | bytes 262144 | tf_op jit(solution)/shard_map/all_to_all | solution.py:255
  128.5 0.0 copy-done.1
  128.5 0.0 copy-done.2
  128.5 0.8 transform_a.1
  129.4 2.0 %collective-permute-start = (bf16[256,256]{1,0:T(8,128)(2,1)S(1)}, bf16[256,256]{1,0:T(8,128)(2,1)S(1)}, u32[]{:S(2)}, u32[]{:S(2)}) collective-permute-start(bf16[256,256]{1,0:T(8,128)(2,1)S(1)} %get-tuple-element.12), channel_id=1, source_target_pairs={{0,1},{1,0},{2,3},{3,2},{4,5},{5,4},{6,7},{7,6},{8,9},{9,8},{10,11... | collective-permute-start | bytes 393224 | tf_op jit(solution)/shard_map/ppermute | solution.py:266
  131.3 1.3 collective-permute-done.got_ref
  132.7 0.0 copy-done.3
  132.7 0.8 transform_b.1
  133.4 18.6 %all_to_all.22 = bf16[32,16,128]{2,1,0:T(8,128)(2,1)S(1)} all-to-all(bf16[32,16,128]{2,1,0:T(8,128)(2,1)S(1)} %bitcast.11), channel_id=1, replica_groups={{0,2,4,6,8,10,12,14,16,18,20,22,24,26,28,30},{1,3,5,7,9,11,13,15,17,19,..., dimensions={0} | all-to-all | bytes 262144 | tf_op jit(solution)/shard_map/all_to_all | solution.py:255
  152.1 17.6 %all_to_all.23 = bf16[16,32,128]{2,1,0:T(8,128)(2,1)S(1)} all-to-all(bf16[16,32,128]{2,1,0:T(8,128)(2,1)S(1)} %copy.15), channel_id=1, replica_groups=mesh['grp'=2,'row'=16,'col'=32] {'row'}, dimensions={0} | all-to-all | bytes 262144 | tf_op jit(solution)/shard_map/all_to_all | solution.py:252
  169.7 0.0 copy-done
  169.7 0.0 copy-done.4
  169.7 1.3 merge_out.1
  (1 shorter events, 0.0 us)
Async XLA Ops:
  0.0 128.5 %copy-start.1 = (f32[2,2,2,128,128]{4,3,2,1,0:T(8,128)S(1)}, f32[2,2,2,128,128]{4,3,2,1,0:T(8,128)}, u32[]{:S(2)}) copy-start(f32[2,2,2,128,128]{4,3,2,1,0:T(8,128)} %constant.53.clone.turn_ref) | copy-start | bytes 1572868
  0.0 128.5 %copy-start.2 = (bf16[2,256,256]{2,1,0:T(8,128)(2,1)S(1)}, bf16[2,256,256]{2,1,0:T(8,128)(2,1)}, u32[]{:S(2)}) copy-start(bf16[2,256,256]{2,1,0:T(8,128)(2,1)} %constant.52.clone.first_ref) | copy-start | bytes 786436
  0.1 132.6 %copy-start.3 = (bf16[2,256,256]{2,1,0:T(8,128)(2,1)S(1)}, bf16[2,256,256]{2,1,0:T(8,128)(2,1)}, u32[]{:S(2)}) copy-start(bf16[2,256,256]{2,1,0:T(8,128)(2,1)} %constant.54.clone.last_ref) | copy-start | bytes 786436
  3.5 166.2 %copy-start = (bf16[512,2048]{1,0:T(8,128)(2,1)S(1)}, bf16[512,2048]{1,0:T(8,128)(2,1)}, u32[]{:S(2)}) copy-start(bf16[512,2048]{1,0:T(8,128)(2,1)} %w_ref.1) | copy-start | bytes 6291460
  3.5 166.2 %copy-start.4 = (bf16[128,128]{1,0:T(8,128)(2,1)S(1)}, bf16[128,128]{1,0:T(8,128)(2,1)}, u32[]{:S(2)}) copy-start(bf16[128,128]{1,0:T(8,128)(2,1)} %constant.55.clone.merge_ref) | copy-start | bytes 98308
  129.4 3.3 %collective-permute-start = (bf16[256,256]{1,0:T(8,128)(2,1)S(1)}, bf16[256,256]{1,0:T(8,128)(2,1)S(1)}, u32[]{:S(2)}, u32[]{:S(2)}) collective-permute-start(bf16[256,256]{1,0:T(8,128)(2,1)S(1)} %get-tuple-element.12), channel_id=1, source_target_pairs={{0,1},{1,0},{2,3},{3,2},{4,5},{5,4},{6,7},{7,6},{8,9},{9,8},{10,11... | collective-permute-start | bytes 393224 | tf_op jit(solution)/shard_map/ppermute | solution.py:266

commit v3 on v2

--- a/solution.py
+++ b/solution.py
@@ -52,7 +52,7 @@
     def halves(table):
         return [table[..., h * toks : (h + 1) * toks] for h in range(CORES)]
 
-    first = np.stack([np.concatenate([np.cos(t), -np.sin(t)], axis=1) for t in halves(first)])
+    first = np.concatenate([f(t) for t in halves(first) for f in (np.cos, lambda v: -np.sin(v))], axis=1)
     turn = np.stack(
         [
             np.stack([np.stack([np.cos(t), -np.sin(t)]) * scale for t in halves(turn[c * toks : (c + 1) * toks])])
@@ -63,7 +63,9 @@
     return first, turn, last
 
 
-def project(tok_hbm, gain_hbm, w_hbm, spread_hbm, out_ref, tok_v, w_v, gain_v, spread_v, sems, small_sems):
+def project(
+    tok_hbm, gain_hbm, w_hbm, spread_hbm, out_hbm, tok_v, w_v, gain_v, spread_v, out_v, sems, small_sems, out_sems
+):
     toks, width = tok_v.shape
     part = width // CHUNKS
     small = [
@@ -99,38 +101,52 @@
     factor = lax.rsqrt(squares * (1.0 / width) + NORM_EPS)
     mixin = (total * factor).astype(BF16)
     small[1].wait()
+    leaving = []
     for g in range(w_v.shape[1] // GROUP_CH):
         at = slice(g * GROUP_CH, (g + 1) * GROUP_CH)
-        out_ref[at, :] = lax.dot_general(
+        out_v[at, :] = lax.dot_general(
             spread_v[...], mixin[:, at], (((0,), (1,)), ((), ())), preferred_element_type=F32
         ).astype(BF16)
-
-
-def transform_a(which_ref, x_ref, first_ref, turn_ref, own_ref, send_ref):
+        rows = pl.ds(g * GROUP_CH, GROUP_CH)
+        leaving.append(pltpu.make_async_copy(out_v.at[rows, :], out_hbm.at[rows, :], out_sems.at[g]))
+        leaving[-1].start()
+    for copy in leaving:
+        copy.wait()
+
+
+def transform_a(x_ref, first_ref, turn_ref, own_ref, send_ref):
     chips, _, rows, toks = x_ref.shape
-    core = which_ref[0]
-    for half, ref in ((core, own_ref), (1 - core, send_ref)):
-        table = first_ref[half]
-        w_re, w_im = turn_ref[core, half, 0], turn_ref[core, half, 1]
-        for j in range(CORES):
-            sine = which_ref[1 + j] == 1
-            y = lax.dot_general(
-                x_ref[:, j].reshape(chips * rows, toks),
-                table,
-                (((0,), (0,)), ((), ())),
-                preferred_element_type=F32,
-            )
-            y_re, y_im = y[:, :toks], y[:, toks:]
+    cols = chips * CORES
+    col = lax.axis_index("col")
+    core = lax.rem(col, CORES)
+    feature = lax.axis_index("row") * cols + (col - core)
+    low = core == 0
+    for j in range(CORES):
+        sine = lax.rem(feature + j, GROUP_CH) > GROUP_CH // 2
+        y = lax.dot_general(
+            x_ref[:, j].reshape(chips * rows, toks),
+            first_ref[...],
+            (((0,), (0,)), ((), ())),
+            preferred_element_type=F32,
+        )
+        halves = []
+        for h in range(CORES):
+            y_re = y[:, 2 * h * toks : (2 * h + 1) * toks]
+            y_im = y[:, (2 * h + 1) * toks : (2 * h + 2) * toks]
+            w_re, w_im = turn_ref[core, h, 0], turn_ref[core, h, 1]
             u_re = (y_re * w_re - y_im * w_im).astype(BF16)
             u_im = (y_re * w_im + y_im * w_re).astype(BF16)
-            at = slice(j * toks, (j + 1) * toks)
-            ref[:toks, at] = jnp.where(sine, -u_im, u_re)
-            ref[toks:, at] = jnp.where(sine, u_re, u_im)
-
-
-def transform_b(which_ref, own_ref, got_ref, last_ref, out_ref):
+            halves.append((jnp.where(sine, -u_im, u_re), jnp.where(sine, u_re, u_im)))
+        at = slice(j * toks, (j + 1) * toks)
+        for k in range(2):
+            part = slice(k * toks, (k + 1) * toks)
+            own_ref[part, at] = jnp.where(low, halves[0][k], halves[1][k])
+            send_ref[part, at] = jnp.where(low, halves[1][k], halves[0][k])
+
+
+def transform_b(own_ref, got_ref, last_ref, out_ref):
     chips, _, rows, toks = out_ref.shape
-    core = which_ref[0]
+    core = lax.rem(lax.axis_index("col"), CORES)
     z = jnp.dot(last_ref[core], own_ref[...], preferred_element_type=F32)
     z += jnp.dot(last_ref[1 - core], got_ref[...], preferred_element_type=F32)
     z = z.astype(BF16)
@@ -168,7 +184,6 @@
 
 
 VMEM = pl.BlockSpec(memory_space=pltpu.VMEM)
-SMEM = pl.BlockSpec(memory_space=pltpu.SMEM)
 HBM = pl.BlockSpec(memory_space=pltpu.HBM)
 
 
@@ -179,42 +194,44 @@
         project,
         out_shape=jax.ShapeDtypeStruct((feats, toks), BF16),
         in_specs=[HBM, HBM, HBM, HBM],
-        out_specs=VMEM,
+        out_specs=HBM,
         scratch_shapes=[
             pltpu.VMEM((toks, width), BF16),
             pltpu.VMEM((width, feats), BF16),
             pltpu.VMEM(norm_gain.shape, BF16),
             pltpu.VMEM(spread.shape, BF16),
+            pltpu.VMEM((feats, toks), BF16),
             pltpu.SemaphoreType.DMA((2, CHUNKS)),
             pltpu.SemaphoreType.DMA((2,)),
+            pltpu.SemaphoreType.DMA((feats // GROUP_CH,)),
         ],
         compiler_params=pltpu.CompilerParams(vmem_limit_bytes=PROJECT_LIMIT),
         name="project",
     )(tokens, norm_gain, w_in, spread)
 
 
-def call_transform_a(which, x, first, turn):
+def call_transform_a(x, first, turn):
     toks = x.shape[-1]
     half = jax.ShapeDtypeStruct((2 * toks, CORES * toks), BF16)
     return pl.pallas_call(
         transform_a,
         out_shape=(half, half),
-        in_specs=[SMEM, VMEM, VMEM, VMEM],
+        in_specs=[VMEM, VMEM, VMEM],
         out_specs=(VMEM, VMEM),
         compiler_params=pltpu.CompilerParams(vmem_limit_bytes=VMEM_LIMIT),
         name="transform_a",
-    )(which, x, first, turn)
-
-
-def call_transform_b(which, own, got, last, shape):
+    )(x, first, turn)
+
+
+def call_transform_b(own, got, last, shape):
     return pl.pallas_call(
         transform_b,
         out_shape=jax.ShapeDtypeStruct(shape, BF16),
-        in_specs=[SMEM, VMEM, VMEM, VMEM],
+        in_specs=[VMEM, VMEM, VMEM],
         out_specs=VMEM,
         compiler_params=pltpu.CompilerParams(vmem_limit_bytes=VMEM_LIMIT),
         name="transform_b",
-    )(which, own, got, last)
+    )(own, got, last)
 
 
 def call_merge_out(x, merge, w_out):
@@ -240,14 +257,6 @@
     lines = [[CORES * y + c for y in range(chips)] for c in range(CORES)]
     pairs = [(i, i ^ 1) for i in range(cols)]
 
-    col = lax.axis_index("col")
-    core = col % CORES
-    feature = lax.axis_index("row") * cols + (col - core)
-    which = jnp.stack(
-        [core] + [((feature + j) % GROUP_CH > GROUP_CH // 2).astype(jnp.int32) for j in range(CORES)]
-    )
-    which, tokens = lax.optimization_barrier((which, tokens))
-
     def along_row(x):
         return lax.all_to_all(x, "row", split_axis=0, concat_axis=0, tiled=True)
 
@@ -261,10 +270,10 @@
     sent = along_line(sent.transpose(1, 0, 2))
     shape = (chips, CORES, rows, toks)
     own, give = call_transform_a(
-        which, sent.reshape(shape), jnp.asarray(first, BF16), jnp.asarray(turn, F32)
+        sent.reshape(shape), jnp.asarray(first, BF16), jnp.asarray(turn, F32)
     )
     got = lax.ppermute(give, "col", pairs)
-    back = call_transform_b(which, own, got, jnp.asarray(last, BF16), shape)
+    back = call_transform_b(own, got, jnp.asarray(last, BF16), shape)
     back = along_line(back.reshape(cols, rows, toks))
     back = along_row(back.transpose(1, 0, 2))
     return call_merge_out(back.reshape(feats, toks), jnp.asarray(merge, BF16), w_out)

time: 172 us -> 170 us (0.988)
  no operation moved by 1% of the time
where the time goes in v3:
time: 170 us
  blocking collectives  161 us (95%)
  Pallas kernels  5.23 us (3%)
  starting transfers between devices  1.95 us (1%)
    all_to_all x2, blocking collectives, along_row(): return lax.all_to_all(x, 'row', split_axis=0, concat_axis=0, tiled=True)  115 us
    all_to_all x2, blocking collectives, along_line(): lax.all_to_all(x, 'col', split_axis=0, concat_axis=0, tiled=True, axis_in...  45.7 us
    pallas_call x1, Pallas kernels, call_project(): pl.pallas_call(project, out_shape=jax.ShapeDtypeStruct((feats, toks), BF1...  3.43 us
  transfers between devices with their start and end apart: 1, of which 1 were waited for; matrix products, arithmetic and copies ran while one was open for 0% of the time, Pallas kernels for 0%

profile of v3, /device:TPU:6, one launch (start us, length us, event | category | flops | bytes accessed | tf_op | source)
XLA Modules:
  0.0 169.8 jit_solution(167321442305997503)
XLA Ops:
  0.0 0.0 copy-start.1
  0.0 0.0 copy-start.2
  0.0 0.0 copy-start.3
  0.0 3.4 %project.1 = bf16[512,128]{1,0:T(8,128)(2,1)} custom-call(bf16[1,128,2048]{2,1,0:T(8,128)(2,1)} %tok_hbm.1, bf16[2048]{0:T(1024)(128)(2,1)} %gain_hbm.1, bf16[2048,512]{1,0:T(8,128)(2,1)} %w_hbm.1, bf16[128,128]{1,0:T(8,128)(2,1)} %constant.10.clone.spread_hbm), custom_call_target="tpu_custom_call" | custom-call | tf_op jit(solution)/shard_map/project/pallas_call | solution.py:193
  3.4 0.0 copy-start
  3.5 0.0 copy-start.4
  3.5 97.9 %all_to_all.20 = bf16[16,32,128]{2,1,0:T(8,128)(2,1)S(1)} all-to-all(bf16[16,32,128]{2,1,0:T(8,128)(2,1)} %bitcast.9), channel_id=1, replica_groups=mesh['grp'=2,'row'=16,'col'=32] {'row'}, dimensions={0} | all-to-all | bytes 262144 | tf_op jit(solution)/shard_map/all_to_all | solution.py:261
  101.3 0.1 copy.14
  101.4 27.1 %all_to_all.21 = bf16[32,16,128]{2,1,0:T(8,128)(2,1)S(1)} all-to-all(bf16[32,16,128]{2,1,0:T(8,128)(2,1)S(1)} %copy.14), channel_id=1, replica_groups={{0,2,4,6,8,10,12,14,16,18,20,22,24,26,28,30},{1,3,5,7,9,11,13,15,17,19,..., dimensions={0} | all-to-all | bytes 262144 | tf_op jit(solution)/shard_map/all_to_all | solution.py:264
  128.5 0.0 copy-done.1
  128.5 0.0 copy-done.2
  128.5 0.3 transform_a.1
  128.8 2.0 %collective-permute-start = (bf16[256,256]{1,0:T(8,128)(2,1)S(1)}, bf16[256,256]{1,0:T(8,128)(2,1)S(1)}, u32[]{:S(2)}, u32[]{:S(2)}) collective-permute-start(bf16[256,256]{1,0:T(8,128)(2,1)S(1)} %get-tuple-element.8), channel_id=1, source_target_pairs={{0,1},{1,0},{2,3},{3,2},{4,5},{5,4},{6,7},{7,6},{8,9},{9,8},{10,11... | collective-permute-start | bytes 393224 | tf_op jit(solution)/shard_map/ppermute | solution.py:275
  130.7 1.3 collective-permute-done.got_ref
  132.1 0.0 copy-done.3
  132.1 0.2 transform_b.1
  132.3 18.6 %all_to_all.22 = bf16[32,16,128]{2,1,0:T(8,128)(2,1)S(1)} all-to-all(bf16[32,16,128]{2,1,0:T(8,128)(2,1)S(1)} %bitcast.7), channel_id=1, replica_groups={{0,2,4,6,8,10,12,14,16,18,20,22,24,26,28,30},{1,3,5,7,9,11,13,15,17,19,..., dimensions={0} | all-to-all | bytes 262144 | tf_op jit(solution)/shard_map/all_to_all | solution.py:264
  150.9 17.6 %all_to_all.23 = bf16[16,32,128]{2,1,0:T(8,128)(2,1)S(1)} all-to-all(bf16[16,32,128]{2,1,0:T(8,128)(2,1)S(1)} %copy.15), channel_id=1, replica_groups=mesh['grp'=2,'row'=16,'col'=32] {'row'}, dimensions={0} | all-to-all | bytes 262144 | tf_op jit(solution)/shard_map/all_to_all | solution.py:261
  168.5 0.0 copy-done
  168.6 0.0 copy-done.4
  168.6 1.3 merge_out.1
  (1 shorter events, 0.0 us)
Async XLA Ops:
  0.0 128.5 %copy-start.1 = (f32[2,2,2,128,128]{4,3,2,1,0:T(8,128)S(1)}, f32[2,2,2,128,128]{4,3,2,1,0:T(8,128)}, u32[]{:S(2)}) copy-start(f32[2,2,2,128,128]{4,3,2,1,0:T(8,128)} %constant.12.clone.turn_ref) | copy-start | bytes 1572868
  0.0 128.5 %copy-start.2 = (bf16[256,512]{1,0:T(8,128)(2,1)S(1)}, bf16[256,512]{1,0:T(8,128)(2,1)}, u32[]{:S(2)}) copy-start(bf16[256,512]{1,0:T(8,128)(2,1)} %constant.11.clone.first_ref) | copy-start | bytes 786436
  0.0 132.1 %copy-start.3 = (bf16[2,256,256]{2,1,0:T(8,128)(2,1)S(1)}, bf16[2,256,256]{2,1,0:T(8,128)(2,1)}, u32[]{:S(2)}) copy-start(bf16[2,256,256]{2,1,0:T(8,128)(2,1)} %constant.13.clone.last_ref) | copy-start | bytes 786436
  3.4 165.1 %copy-start = (bf16[512,2048]{1,0:T(8,128)(2,1)S(1)}, bf16[512,2048]{1,0:T(8,128)(2,1)}, u32[]{:S(2)}) copy-start(bf16[512,2048]{1,0:T(8,128)(2,1)} %w_ref.1) | copy-start | bytes 6291460
  3.5 165.1 %copy-start.4 = (bf16[128,128]{1,0:T(8,128)(2,1)S(1)}, bf16[128,128]{1,0:T(8,128)(2,1)}, u32[]{:S(2)}) copy-start(bf16[128,128]{1,0:T(8,128)(2,1)} %constant.14.clone.merge_ref) | copy-start | bytes 98308
  128.8 3.3 %collective-permute-start = (bf16[256,256]{1,0:T(8,128)(2,1)S(1)}, bf16[256,256]{1,0:T(8,128)(2,1)S(1)}, u32[]{:S(2)}, u32[]{:S(2)}) collective-permute-start(bf16[256,256]{1,0:T(8,128)(2,1)S(1)} %get-tuple-element.8), channel_id=1, source_target_pairs={{0,1},{1,0},{2,3},{3,2},{4,5},{5,4},{6,7},{7,6},{8,9},{9,8},{10,11... | collective-permute-start | bytes 393224 | tf_op jit(solution)/shard_map/ppermute | solution.py:275

commit v4 on v3

--- a/solution.py
+++ b/solution.py
@@ -12,7 +12,8 @@
 GROUP_CH = 128
 NORM_EPS = 1e-06
 CORES = 2
-CHUNKS = 4
+IN_PARTS = 2
+OUT_PARTS = 4
 VMEM_LIMIT = 16 * 1024 * 1024
 PROJECT_LIMIT = 60 * 1024 * 1024
 
@@ -63,17 +64,15 @@
     return first, turn, last
 
 
-def project(
-    tok_hbm, gain_hbm, w_hbm, spread_hbm, out_hbm, tok_v, w_v, gain_v, spread_v, out_v, sems, small_sems, out_sems
-):
+def project(tok_hbm, gain_hbm, w_hbm, spread_hbm, out_ref, tok_v, w_v, gain_v, spread_v, sems, small_sems):
     toks, width = tok_v.shape
-    part = width // CHUNKS
+    part = width // IN_PARTS
     small = [
         pltpu.make_async_copy(gain_hbm, gain_v, small_sems.at[0]),
         pltpu.make_async_copy(spread_hbm, spread_v, small_sems.at[1]),
     ]
     copies = []
-    for j in range(CHUNKS):
+    for j in range(IN_PARTS):
         at = pl.ds(j * part, part)
         copies.append(
             (
@@ -90,7 +89,7 @@
     gain = gain_v[...].astype(F32).reshape(1, width)
     squares = jnp.zeros((toks, 1), F32)
     total = jnp.zeros((toks, w_v.shape[1]), F32)
-    for j in range(CHUNKS):
+    for j in range(IN_PARTS):
         at = slice(j * part, (j + 1) * part)
         copies[j][0].wait()
         x = tok_v[:, at].astype(F32)
@@ -101,17 +100,11 @@
     factor = lax.rsqrt(squares * (1.0 / width) + NORM_EPS)
     mixin = (total * factor).astype(BF16)
     small[1].wait()
-    leaving = []
     for g in range(w_v.shape[1] // GROUP_CH):
         at = slice(g * GROUP_CH, (g + 1) * GROUP_CH)
-        out_v[at, :] = lax.dot_general(
+        out_ref[at, :] = lax.dot_general(
             spread_v[...], mixin[:, at], (((0,), (1,)), ((), ())), preferred_element_type=F32
         ).astype(BF16)
-        rows = pl.ds(g * GROUP_CH, GROUP_CH)
-        leaving.append(pltpu.make_async_copy(out_v.at[rows, :], out_hbm.at[rows, :], out_sems.at[g]))
-        leaving[-1].start()
-    for copy in leaving:
-        copy.wait()
 
 
 def transform_a(x_ref, first_ref, turn_ref, own_ref, send_ref):
@@ -166,9 +159,9 @@
             ).astype(BF16)
         )
     spectrum = jnp.concatenate(pieces, axis=1)
-    part = width // CHUNKS
+    part = width // OUT_PARTS
     copies = []
-    for j in range(CHUNKS):
+    for j in range(OUT_PARTS):
         at = slice(j * part, (j + 1) * part)
         out_v[:, at] = jnp.dot(spectrum, w_ref[:, at], preferred_element_type=F32).astype(BF16)
         copies.append(
@@ -192,18 +185,16 @@
     feats = w_in.shape[1]
     return pl.pallas_call(
         project,
-        out_shape=jax.ShapeDtypeStruct((feats, toks), BF16),
+        out_shape=pltpu.VMEM((feats, toks), BF16),
         in_specs=[HBM, HBM, HBM, HBM],
-        out_specs=HBM,
+        out_specs=VMEM,
         scratch_shapes=[
             pltpu.VMEM((toks, width), BF16),
             pltpu.VMEM((width, feats), BF16),
             pltpu.VMEM(norm_gain.shape, BF16),
             pltpu.VMEM(spread.shape, BF16),
-            pltpu.VMEM((feats, toks), BF16),
-            pltpu.SemaphoreType.DMA((2, CHUNKS)),
+            pltpu.SemaphoreType.DMA((2, IN_PARTS)),
             pltpu.SemaphoreType.DMA((2,)),
-            pltpu.SemaphoreType.DMA((feats // GROUP_CH,)),
         ],
         compiler_params=pltpu.CompilerParams(vmem_limit_bytes=PROJECT_LIMIT),
         name="project",
@@ -242,7 +233,7 @@
         out_shape=jax.ShapeDtypeStruct((1, toks, width), BF16),
         in_specs=[VMEM, VMEM, VMEM],
         out_specs=HBM,
-        scratch_shapes=[pltpu.VMEM((toks, width), BF16), pltpu.SemaphoreType.DMA((CHUNKS,))],
+        scratch_shapes=[pltpu.VMEM((toks, width), BF16), pltpu.SemaphoreType.DMA((OUT_PARTS,))],
         compiler_params=pltpu.CompilerParams(vmem_limit_bytes=VMEM_LIMIT),
         name="merge_out",
     )(x, merge, w_out)

time: 170 us -> 169 us (level)
  no operation moved by 1% of the time
where the time goes in v4:
time: 169 us
  blocking collectives  161 us (95%)
  Pallas kernels  4.35 us (3%)
  starting transfers between devices  1.95 us (1%)
    all_to_all x2, blocking collectives, along_row(): return lax.all_to_all(x, 'row', split_axis=0, concat_axis=0, tiled=True)  115 us
    all_to_all x2, blocking collectives, along_line(): lax.all_to_all(x, 'col', split_axis=0, concat_axis=0, tiled=True, axis_in...  45.7 us
  transfers between devices with their start and end apart: 1, of which 1 were waited for; matrix products, arithmetic and copies ran while one was open for 0% of the time, Pallas kernels for 0%

profile of v4, /device:TPU:6, one launch (start us, length us, event | category | flops | bytes accessed | tf_op | source)
XLA Modules:
  0.0 168.7 jit_solution(11793507529816444348)
XLA Ops:
  0.0 0.0 copy-start.1
  0.0 0.0 copy-start.2
  0.0 0.0 copy-start.3
  0.0 2.5 %project.1 = bf16[512,128]{1,0:T(8,128)(2,1)S(1)} custom-call(bf16[1,128,2048]{2,1,0:T(8,128)(2,1)} %tok_hbm.1, bf16[2048]{0:T(1024)(128)(2,1)} %gain_hbm.1, bf16[2048,512]{1,0:T(8,128)(2,1)} %w_hbm.1, bf16[128,128]{1,0:T(8,128)(2,1)} %constant.10.clone.spread_hbm), custom_call_target="tpu_custom_call" | custom-call | tf_op jit(solution)/shard_map/project/pallas_call | solution.py:186
  2.6 0.0 copy-start
  2.6 0.0 copy-start.4
  2.6 97.6 %all_to_all.20 = bf16[16,32,128]{2,1,0:T(8,128)(2,1)S(1)} all-to-all(bf16[16,32,128]{2,1,0:T(8,128)(2,1)S(1)} %bitcast.9), channel_id=1, replica_groups=mesh['grp'=2,'row'=16,'col'=32] {'row'}, dimensions={0} | all-to-all | bytes 262144 | tf_op jit(solution)/shard_map/all_to_all | solution.py:252
  100.2 0.1 copy.14
  100.3 27.1 %all_to_all.21 = bf16[32,16,128]{2,1,0:T(8,128)(2,1)S(1)} all-to-all(bf16[32,16,128]{2,1,0:T(8,128)(2,1)S(1)} %copy.14), channel_id=1, replica_groups={{0,2,4,6,8,10,12,14,16,18,20,22,24,26,28,30},{1,3,5,7,9,11,13,15,17,19,..., dimensions={0} | all-to-all | bytes 262144 | tf_op jit(solution)/shard_map/all_to_all | solution.py:255
  127.4 0.0 copy-done.1
  127.4 0.0 copy-done.2
  127.4 0.3 transform_a.1
  127.7 2.0 %collective-permute-start = (bf16[256,256]{1,0:T(8,128)(2,1)S(1)}, bf16[256,256]{1,0:T(8,128)(2,1)S(1)}, u32[]{:S(2)}, u32[]{:S(2)}) collective-permute-start(bf16[256,256]{1,0:T(8,128)(2,1)S(1)} %get-tuple-element.8), channel_id=1, source_target_pairs={{0,1},{1,0},{2,3},{3,2},{4,5},{5,4},{6,7},{7,6},{8,9},{9,8},{10,11... | collective-permute-start | bytes 393224 | tf_op jit(solution)/shard_map/ppermute | solution.py:266
  129.6 1.3 collective-permute-done.got_ref
  131.0 0.0 copy-done.3
  131.0 0.2 transform_b.1
  131.2 18.6 %all_to_all.22 = bf16[32,16,128]{2,1,0:T(8,128)(2,1)S(1)} all-to-all(bf16[32,16,128]{2,1,0:T(8,128)(2,1)S(1)} %bitcast.7), channel_id=1, replica_groups={{0,2,4,6,8,10,12,14,16,18,20,22,24,26,28,30},{1,3,5,7,9,11,13,15,17,19,..., dimensions={0} | all-to-all | bytes 262144 | tf_op jit(solution)/shard_map/all_to_all | solution.py:255
  149.8 17.6 %all_to_all.23 = bf16[16,32,128]{2,1,0:T(8,128)(2,1)S(1)} all-to-all(bf16[16,32,128]{2,1,0:T(8,128)(2,1)S(1)} %copy.15), channel_id=1, replica_groups=mesh['grp'=2,'row'=16,'col'=32] {'row'}, dimensions={0} | all-to-all | bytes 262144 | tf_op jit(solution)/shard_map/all_to_all | solution.py:252
  167.4 0.0 copy-done
  167.4 0.0 copy-done.4
  167.4 1.3 merge_out.1
  (1 shorter events, 0.0 us)
Async XLA Ops:
  0.0 127.4 %copy-start.1 = (f32[2,2,2,128,128]{4,3,2,1,0:T(8,128)S(1)}, f32[2,2,2,128,128]{4,3,2,1,0:T(8,128)}, u32[]{:S(2)}) copy-start(f32[2,2,2,128,128]{4,3,2,1,0:T(8,128)} %constant.12.clone.turn_ref) | copy-start | bytes 1572868
  0.0 127.4 %copy-start.2 = (bf16[256,512]{1,0:T(8,128)(2,1)S(1)}, bf16[256,512]{1,0:T(8,128)(2,1)}, u32[]{:S(2)}) copy-start(bf16[256,512]{1,0:T(8,128)(2,1)} %constant.11.clone.first_ref) | copy-start | bytes 786436
  0.0 131.0 %copy-start.3 = (bf16[2,256,256]{2,1,0:T(8,128)(2,1)S(1)}, bf16[2,256,256]{2,1,0:T(8,128)(2,1)}, u32[]{:S(2)}) copy-start(bf16[2,256,256]{2,1,0:T(8,128)(2,1)} %constant.13.clone.last_ref) | copy-start | bytes 786436
  2.6 164.9 %copy-start = (bf16[512,2048]{1,0:T(8,128)(2,1)S(1)}, bf16[512,2048]{1,0:T(8,128)(2,1)}, u32[]{:S(2)}) copy-start(bf16[512,2048]{1,0:T(8,128)(2,1)} %w_ref.1) | copy-start | bytes 6291460
  2.6 164.9 %copy-start.4 = (bf16[128,128]{1,0:T(8,128)(2,1)S(1)}, bf16[128,128]{1,0:T(8,128)(2,1)}, u32[]{:S(2)}) copy-start(bf16[128,128]{1,0:T(8,128)(2,1)} %constant.14.clone.merge_ref) | copy-start | bytes 98308
  127.7 3.3 %collective-permute-start = (bf16[256,256]{1,0:T(8,128)(2,1)S(1)}, bf16[256,256]{1,0:T(8,128)(2,1)S(1)}, u32[]{:S(2)}, u32[]{:S(2)}) collective-permute-start(bf16[256,256]{1,0:T(8,128)(2,1)S(1)} %get-tuple-element.8), channel_id=1, source_target_pairs={{0,1},{1,0},{2,3},{3,2},{4,5},{5,4},{6,7},{7,6},{8,9},{9,8},{10,11... | collective-permute-start | bytes 393224 | tf_op jit(solution)/shard_map/ppermute | solution.py:266

commit v5 on v4

--- a/solution.py
+++ b/solution.py
@@ -42,26 +42,26 @@
     low = CORES * toks
     high = rows * chips
     assert high == low
-    a = (np.arange(rows)[None, :] * chips + np.arange(chips)[:, None]).reshape(-1)
-    k1 = np.arange(high)
+    a = np.arange(high)
     b = np.arange(low)
-    first = 2.0 * np.pi * (a[:, None] * k1[None, :] % high) / high
-    turn = 2.0 * np.pi * (b[:, None] * k1[None, :] % length) / length
+    first = 2.0 * np.pi * (a[:, None] * a[None, :] % high) / high
+    turn = 2.0 * np.pi * (b[:, None] * a[None, :] % length) / length
     last = 2.0 * np.pi * (a[:, None] * b[None, :] % low) / low
     scale = 1.0 / math.sqrt(length * GROUP_CH)
-
-    def halves(table):
-        return [table[..., h * toks : (h + 1) * toks] for h in range(CORES)]
-
-    first = np.concatenate([f(t) for t in halves(first) for f in (np.cos, lambda v: -np.sin(v))], axis=1)
-    turn = np.stack(
-        [
-            np.stack([np.stack([np.cos(t), -np.sin(t)]) * scale for t in halves(turn[c * toks : (c + 1) * toks])])
-            for c in range(CORES)
-        ]
-    )
-    last = np.stack([np.concatenate([np.cos(t), np.sin(t)], axis=1) for t in halves(last)])
-    return first, turn, last
+    spread = np.zeros((high, CORES, 2, toks))
+    gather = np.zeros((CORES, high, 2, toks))
+    turns = np.zeros((CORES, CORES, 2, toks, toks))
+    for h in range(CORES):
+        at = slice(h * toks, (h + 1) * toks)
+        spread[:, h, 0] = np.cos(first[:, at])
+        spread[:, h, 1] = -np.sin(first[:, at])
+        gather[h, :, 0] = np.cos(last[:, at])
+        gather[h, :, 1] = np.sin(last[:, at])
+        for c in range(CORES):
+            angle = turn[c * toks : (c + 1) * toks, at]
+            turns[c, h, 0] = np.cos(angle) * scale
+            turns[c, h, 1] = -np.sin(angle) * scale
+    return spread.reshape(high, -1), turns, gather.reshape(CORES, high, -1)
 
 
 def project(tok_hbm, gain_hbm, w_hbm, spread_hbm, out_ref, tok_v, w_v, gain_v, spread_v, sems, small_sems):
@@ -107,44 +107,42 @@
         ).astype(BF16)
 
 
-def transform_a(x_ref, first_ref, turn_ref, own_ref, send_ref):
-    chips, _, rows, toks = x_ref.shape
-    cols = chips * CORES
-    col = lax.axis_index("col")
-    core = lax.rem(col, CORES)
-    feature = lax.axis_index("row") * cols + (col - core)
+def transform_a(x_ref, first_ref, turn_ref, own_ref, send_ref, wide):
+    count, toks = x_ref.shape
+    wide[...] = x_ref[...].astype(F32)
+    core = lax.axis_index("core")
+    feature = (lax.axis_index("row") * lax.axis_size("y") + lax.axis_index("y")) * CORES
     low = core == 0
     for j in range(CORES):
+        x = wide[pl.ds(j, count // CORES, stride=CORES), :].astype(BF16)
+        y = lax.dot_general(
+            x, first_ref[...], (((0,), (0,)), ((), ())), preferred_element_type=F32
+        )
         sine = lax.rem(feature + j, GROUP_CH) > GROUP_CH // 2
-        y = lax.dot_general(
-            x_ref[:, j].reshape(chips * rows, toks),
-            first_ref[...],
-            (((0,), (0,)), ((), ())),
-            preferred_element_type=F32,
-        )
         halves = []
         for h in range(CORES):
-            y_re = y[:, 2 * h * toks : (2 * h + 1) * toks]
-            y_im = y[:, (2 * h + 1) * toks : (2 * h + 2) * toks]
+            at = 2 * h * toks
+            y_re, y_im = y[:, at : at + toks], y[:, at + toks : at + 2 * toks]
             w_re, w_im = turn_ref[core, h, 0], turn_ref[core, h, 1]
             u_re = (y_re * w_re - y_im * w_im).astype(BF16)
             u_im = (y_re * w_im + y_im * w_re).astype(BF16)
             halves.append((jnp.where(sine, -u_im, u_re), jnp.where(sine, u_re, u_im)))
-        at = slice(j * toks, (j + 1) * toks)
         for k in range(2):
-            part = slice(k * toks, (k + 1) * toks)
-            own_ref[part, at] = jnp.where(low, halves[0][k], halves[1][k])
-            send_ref[part, at] = jnp.where(low, halves[1][k], halves[0][k])
-
-
-def transform_b(own_ref, got_ref, last_ref, out_ref):
-    chips, _, rows, toks = out_ref.shape
-    core = lax.rem(lax.axis_index("col"), CORES)
-    z = jnp.dot(last_ref[core], own_ref[...], preferred_element_type=F32)
-    z += jnp.dot(last_ref[1 - core], got_ref[...], preferred_element_type=F32)
-    z = z.astype(BF16)
+            part = slice((2 * j + k) * toks, (2 * j + k + 1) * toks)
+            own_ref[part, :] = jnp.where(low, halves[0][k], halves[1][k])
+            send_ref[part, :] = jnp.where(low, halves[1][k], halves[0][k])
+
+
+def transform_b(own_ref, got_ref, last_ref, out_ref, wide):
+    core = lax.axis_index("core")
+    count = wide.shape[0] // CORES
+    part = own_ref.shape[0] // CORES
     for j in range(CORES):
-        out_ref[:, j] = z[:, j * toks : (j + 1) * toks].reshape(chips, rows, toks)
+        at = slice(j * part, (j + 1) * part)
+        z = jnp.dot(last_ref[core], own_ref[at, :], preferred_element_type=F32)
+        z += jnp.dot(last_ref[1 - core], got_ref[at, :], preferred_element_type=F32)
+        wide[pl.ds(j, count, stride=CORES), :] = z
+    out_ref[...] = wide[...].astype(BF16)
 
 
 def merge_out(x_ref, merge_ref, w_ref, out_hbm, out_v, sems):
@@ -202,24 +200,26 @@
 
 
 def call_transform_a(x, first, turn):
-    toks = x.shape[-1]
-    half = jax.ShapeDtypeStruct((2 * toks, CORES * toks), BF16)
+    half = jax.ShapeDtypeStruct((2 * CORES * x.shape[1], x.shape[1]), BF16)
     return pl.pallas_call(
         transform_a,
         out_shape=(half, half),
         in_specs=[VMEM, VMEM, VMEM],
         out_specs=(VMEM, VMEM),
+        scratch_shapes=[pltpu.VMEM(x.shape, F32)],
         compiler_params=pltpu.CompilerParams(vmem_limit_bytes=VMEM_LIMIT),
         name="transform_a",
     )(x, first, turn)
 
 
-def call_transform_b(own, got, last, shape):
+def call_transform_b(own, got, last):
+    shape = (CORES * last.shape[1], own.shape[1])
     return pl.pallas_call(
         transform_b,
         out_shape=jax.ShapeDtypeStruct(shape, BF16),
         in_specs=[VMEM, VMEM, VMEM],
         out_specs=VMEM,
+        scratch_shapes=[pltpu.VMEM(shape, F32)],
         compiler_params=pltpu.CompilerParams(vmem_limit_bytes=VMEM_LIMIT),
         name="transform_b",
     )(own, got, last)
@@ -239,42 +239,35 @@
     )(x, merge, w_out)
 
 
-def shards(rows, cols, tokens, norm_gain, w_in, w_out):
+def shards(rows, chips, tokens, norm_gain, w_in, w_out):
     _, toks, width = tokens.shape
     feats = w_in.shape[1]
-    chips = cols // CORES
     spread, merge = channel_tables()
     first, turn, last = sequence_tables(rows, chips, toks)
-    lines = [[CORES * y + c for y in range(chips)] for c in range(CORES)]
-    pairs = [(i, i ^ 1) for i in range(cols)]
-
-    def along_row(x):
-        return lax.all_to_all(x, "row", split_axis=0, concat_axis=0, tiled=True)
-
-    def along_line(x):
-        return lax.all_to_all(
-            x, "col", split_axis=0, concat_axis=0, tiled=True, axis_index_groups=lines
-        )
-
-    sent = call_project(tokens, norm_gain, w_in, jnp.asarray(spread, BF16))
-    sent = along_row(sent.reshape(rows, cols, toks))
-    sent = along_line(sent.transpose(1, 0, 2))
-    shape = (chips, CORES, rows, toks)
-    own, give = call_transform_a(
-        sent.reshape(shape), jnp.asarray(first, BF16), jnp.asarray(turn, F32)
+
+    def exchange(x):
+        x = x.reshape(rows * chips, CORES, toks)
+        x = lax.all_to_all(x, ("row", "y"), split_axis=0, concat_axis=0, tiled=True)
+        return x.reshape(feats, toks)
+
+    sent = exchange(call_project(tokens, norm_gain, w_in, jnp.asarray(spread, BF16)))
+    own, give = call_transform_a(sent, jnp.asarray(first, BF16), jnp.asarray(turn, F32))
+    got = lax.ppermute(give, "core", [(0, 1), (1, 0)])
+    back = exchange(call_transform_b(own, got, jnp.asarray(last, BF16)))
+    return call_merge_out(back, jnp.asarray(merge, BF16), w_out)
+
+
+def solution(mesh):
+    groups, rows, cols = (mesh.shape[name] for name in ("grp", "row", "col"))
+    chips = cols // CORES
+    split = jax.sharding.Mesh(
+        mesh.devices.reshape(groups, rows, chips, CORES), ("grp", "row", "y", "core")
     )
-    got = lax.ppermute(give, "col", pairs)
-    back = call_transform_b(own, got, jnp.asarray(last, BF16), shape)
-    back = along_line(back.reshape(cols, rows, toks))
-    back = along_row(back.transpose(1, 0, 2))
-    return call_merge_out(back.reshape(feats, toks), jnp.asarray(merge, BF16), w_out)
-
-
-def solution(mesh):
+    spec = P("grp", ("row", "y", "core"), None)
     return jax.shard_map(
-        functools.partial(shards, mesh.shape["row"], mesh.shape["col"]),
-        mesh=mesh,
-        in_specs=(P("grp", ("row", "col"), None), P(), P(), P()),
-        out_specs=P("grp", ("row", "col"), None),
+        functools.partial(shards, rows, chips),
+        mesh=split,
+        in_specs=(spec, P(), P(), P()),
+        out_specs=spec,
         check_vma=False,
     )

time: 169 us -> 168 us (level)
    all_to_all x4 -> x2, blocking collectives: 161 us -> 160 us  [exchange(): x = lax.all_to_all(x, ('row', 'y'), split_axis=0, concat_axis=0, tiled=True)]
where the time goes in v5:
time: 168 us
  blocking collectives  160 us (95%)
  Pallas kernels  4.51 us (3%)
  starting transfers between devices  1.95 us (1%)
    all_to_all x2, blocking collectives, exchange(): x = lax.all_to_all(x, ('row', 'y'), split_axis=0, concat_axis=0, tiled=True)  160 us
  transfers between devices with their start and end apart: 1, of which 1 were waited for; matrix products, arithmetic and copies ran while one was open for 0% of the time, Pallas kernels for 0%

profile of v5, /device:TPU:6, one launch (start us, length us, event | category | flops | bytes accessed | tf_op | source)
XLA Modules:
  0.0 168.1 jit_solution(11041333512678359080)
XLA Ops:
  0.0 0.0 copy-start.1
  0.0 0.0 copy-start.2
  0.0 0.0 copy-start.3
  0.0 0.0 copy-start.4
  0.0 0.0 copy-start
  0.0 2.6 %project.1 = bf16[512,128]{1,0:T(8,128)(2,1)S(1)} custom-call(bf16[1,128,2048]{2,1,0:T(8,128)(2,1)} %tok_hbm.1, bf16[2048]{0:T(1024)(128)(2,1)} %gain_hbm.1, bf16[2048,512]{1,0:T(8,128)(2,1)} %w_hbm.1, bf16[128,128]{1,0:T(8,128)(2,1)} %constant.10.clone.spread_hbm), custom_call_target="tpu_custom_call" | custom-call | tf_op jit(solution)/shard_map/project/pallas_call | solution.py:184
  2.6 125.1 %all_to_all.10 = bf16[256,2,128]{2,1,0:T(2,128)(2,1)S(1)} all-to-all(bf16[256,2,128]{2,1,0:T(2,128)(2,1)S(1)} %bitcast.7), channel_id=1, replica_groups=mesh['grp'=2,'row'=16,'y'=16,'core'=2] {'row','y'}, dimensions={0} | all-to-all | bytes 262144 | tf_op jit(solution)/shard_map/all_to_all | solution.py:250
  127.7 0.0 copy-done.1
  127.7 0.0 copy-done.2
  127.7 0.3 transform_a.1
  128.1 2.0 %collective-permute-start = (bf16[512,128]{1,0:T(8,128)(2,1)S(1)}, bf16[512,128]{1,0:T(8,128)(2,1)S(1)}, u32[]{:S(2)}, u32[]{:S(2)}) collective-permute-start(bf16[512,128]{1,0:T(8,128)(2,1)S(1)} %get-tuple-element.8), channel_id=1, source_target_pairs={{0,1},{1,0},{2,3},{3,2},{4,5},{5,4},{6,7},{7,6},{8,9},{9,8},{10,11... | collective-permute-start | bytes 393224 | tf_op jit(solution)/shard_map/ppermute | solution.py:255
  130.0 1.3 collective-permute-done.got_ref
  131.3 0.0 copy-done.3
  131.3 0.3 transform_b.1
  131.6 35.0 %all_to_all.11 = bf16[256,2,128]{2,1,0:T(2,128)(2,1)S(1)} all-to-all(bf16[256,2,128]{2,1,0:T(2,128)(2,1)S(1)} %bitcast.5), channel_id=1, replica_groups=mesh['grp'=2,'row'=16,'y'=16,'core'=2] {'row','y'}, dimensions={0} | all-to-all | bytes 262144 | tf_op jit(solution)/shard_map/all_to_all | solution.py:250
  166.6 0.0 copy-done.4
  166.6 0.0 copy-done
  166.6 1.3 merge_out.1
Async XLA Ops:
  0.0 127.7 %copy-start.1 = (f32[2,2,2,128,128]{4,3,2,1,0:T(8,128)S(1)}, f32[2,2,2,128,128]{4,3,2,1,0:T(8,128)}, u32[]{:S(2)}) copy-start(f32[2,2,2,128,128]{4,3,2,1,0:T(8,128)} %constant.12.clone.turn_ref) | copy-start | bytes 1572868
  0.0 127.7 %copy-start.2 = (bf16[256,512]{1,0:T(8,128)(2,1)S(1)}, bf16[256,512]{1,0:T(8,128)(2,1)}, u32[]{:S(2)}) copy-start(bf16[256,512]{1,0:T(8,128)(2,1)} %constant.11.clone.first_ref) | copy-start | bytes 786436
  0.0 131.3 %copy-start.3 = (bf16[2,256,256]{2,1,0:T(8,128)(2,1)S(1)}, bf16[2,256,256]{2,1,0:T(8,128)(2,1)}, u32[]{:S(2)}) copy-start(bf16[2,256,256]{2,1,0:T(8,128)(2,1)} %constant.13.clone.last_ref) | copy-start | bytes 786436
  0.0 166.6 %copy-start.4 = (bf16[128,128]{1,0:T(8,128)(2,1)S(1)}, bf16[128,128]{1,0:T(8,128)(2,1)}, u32[]{:S(2)}) copy-start(bf16[128,128]{1,0:T(8,128)(2,1)} %constant.14.clone.merge_ref) | copy-start | bytes 98308
  0.0 166.6 %copy-start = (bf16[512,2048]{1,0:T(8,128)(2,1)S(1)}, bf16[512,2048]{1,0:T(8,128)(2,1)}, u32[]{:S(2)}) copy-start(bf16[512,2048]{1,0:T(8,128)(2,1)} %w_ref.1) | copy-start | bytes 6291460
  128.1 3.3 %collective-permute-start = (bf16[512,128]{1,0:T(8,128)(2,1)S(1)}, bf16[512,128]{1,0:T(8,128)(2,1)S(1)}, u32[]{:S(2)}, u32[]{:S(2)}) collective-permute-start(bf16[512,128]{1,0:T(8,128)(2,1)S(1)} %get-tuple-element.8), channel_id=1, source_target_pairs={{0,1},{1,0},{2,3},{3,2},{4,5},{5,4},{6,7},{7,6},{8,9},{9,8},{10,11... | collective-permute-start | bytes 393224 | tf_op jit(solution)/shard_map/ppermute | solution.py:255

commit v6 on v5

--- a/solution.py
+++ b/solution.py
@@ -140,7 +140,7 @@
     for j in range(CORES):
         at = slice(j * part, (j + 1) * part)
         z = jnp.dot(last_ref[core], own_ref[at, :], preferred_element_type=F32)
-        z += jnp.dot(last_ref[1 - core], got_ref[at, :], preferred_element_type=F32)
+        z += jnp.dot(last_ref[1 - core], got_ref[1 - core, at, :], preferred_element_type=F32)
         wide[pl.ds(j, count, stride=CORES), :] = z
     out_ref[...] = wide[...].astype(BF16)
 
@@ -252,7 +252,7 @@
 
     sent = exchange(call_project(tokens, norm_gain, w_in, jnp.asarray(spread, BF16)))
     own, give = call_transform_a(sent, jnp.asarray(first, BF16), jnp.asarray(turn, F32))
-    got = lax.ppermute(give, "core", [(0, 1), (1, 0)])
+    got = lax.all_gather(give, "core")
     back = exchange(call_transform_b(own, got, jnp.asarray(last, BF16)))
     return call_merge_out(back, jnp.asarray(merge, BF16), w_out)
 

time: 168 us -> 167 us (level)
  blocking collectives: 160 us -> 162 us
  starting transfers between devices: 1.95 us -> 0 us
    all_gather x0 -> x1, blocking collectives: none -> 2.05 us  [shards(): got = lax.all_gather(give, 'core')]
    ppermute x1 -> x0, starting transfers between devices: 1.95 us -> none  [shards(): got = lax.ppermute(give, 'core', [(0, 1), (1, 0)])]
  transfers between devices with their start and end apart: 1 -> 0, of which waited for: 1 -> 0; matrix products, arithmetic and copies ran while one was open for 0% -> 0% of each run, Pallas kernels for 0% -> 0%
where the time goes in v6:
time: 167 us
  blocking collectives  162 us (97%)
  Pallas kernels  4.52 us (3%)
    all_to_all x2, blocking collectives, exchange(): x = lax.all_to_all(x, ('row', 'y'), split_axis=0, concat_axis=0, tiled=True)  160 us

profile of v6, /device:TPU:6, one launch (start us, length us, event | category | flops | bytes accessed | tf_op | source)
XLA Modules:
  0.0 166.9 jit_solution(16140838017911164428)
XLA Ops:
  0.0 0.0 copy-start.1
  0.0 0.0 copy-start.3
  0.0 0.0 copy-start.2
  0.0 0.0 copy-start.4
  0.0 0.0 copy-start
  0.0 2.6 %project.1 = bf16[512,128]{1,0:T(8,128)(2,1)S(1)} custom-call(bf16[1,128,2048]{2,1,0:T(8,128)(2,1)} %tok_hbm.1, bf16[2048]{0:T(1024)(128)(2,1)} %gain_hbm.1, bf16[2048,512]{1,0:T(8,128)(2,1)} %w_hbm.1, bf16[128,128]{1,0:T(8,128)(2,1)} %constant.10.clone.spread_hbm), custom_call_target="tpu_custom_call" | custom-call | tf_op jit(solution)/shard_map/project/pallas_call | solution.py:184
  2.6 125.1 %all_to_all.10 = bf16[256,2,128]{2,1,0:T(2,128)(2,1)S(1)} all-to-all(bf16[256,2,128]{2,1,0:T(2,128)(2,1)S(1)} %bitcast.8), channel_id=1, replica_groups=mesh['grp'=2,'row'=16,'y'=16,'core'=2] {'row','y'}, dimensions={0} | all-to-all | bytes 262144 | tf_op jit(solution)/shard_map/all_to_all | solution.py:250
  127.7 0.0 copy-done.1
  127.7 0.0 copy-done.3
  127.7 0.3 transform_a.1
  128.1 2.0 %all-gather = bf16[1024,128]{1,0:T(8,128)(2,1)S(1)} all-gather(bf16[512,128]{1,0:T(8,128)(2,1)S(1)} %get-tuple-element.8), channel_id=2, replica_groups=mesh['grp'=2,'row'=16,'y'=16,'core'=2] {'core'}, dimensions={0}, use_global_device_ids=true | all-gather | bytes 393216 | tf_op jit(solution)/shard_map/all_gather | solution.py:255
  130.1 0.0 copy-done.2
  130.1 0.3 transform_b.1
  130.4 35.0 %all_to_all.11 = bf16[256,2,128]{2,1,0:T(2,128)(2,1)S(1)} all-to-all(bf16[256,2,128]{2,1,0:T(2,128)(2,1)S(1)} %bitcast.9), channel_id=1, replica_groups=mesh['grp'=2,'row'=16,'y'=16,'core'=2] {'row','y'}, dimensions={0} | all-to-all | bytes 262144 | tf_op jit(solution)/shard_map/all_to_all | solution.py:250
  165.4 0.0 copy-done.4
  165.4 0.0 copy-done
  165.4 1.3 merge_out.1
Async XLA Ops:
  0.0 127.7 %copy-start.1 = (f32[2,2,2,128,128]{4,3,2,1,0:T(8,128)S(1)}, f32[2,2,2,128,128]{4,3,2,1,0:T(8,128)}, u32[]{:S(2)}) copy-start(f32[2,2,2,128,128]{4,3,2,1,0:T(8,128)} %constant.12.clone.turn_ref) | copy-start | bytes 1572868
  0.0 127.7 %copy-start.3 = (bf16[256,512]{1,0:T(8,128)(2,1)S(1)}, bf16[256,512]{1,0:T(8,128)(2,1)}, u32[]{:S(2)}) copy-start(bf16[256,512]{1,0:T(8,128)(2,1)} %constant.11.clone.first_ref) | copy-start | bytes 786436
  0.0 130.1 %copy-start.2 = (bf16[2,256,256]{2,1,0:T(8,128)(2,1)S(1)}, bf16[2,256,256]{2,1,0:T(8,128)(2,1)}, u32[]{:S(2)}) copy-start(bf16[2,256,256]{2,1,0:T(8,128)(2,1)} %constant.13.clone.last_ref) | copy-start | bytes 786436
  0.0 165.4 %copy-start.4 = (bf16[128,128]{1,0:T(8,128)(2,1)S(1)}, bf16[128,128]{1,0:T(8,128)(2,1)}, u32[]{:S(2)}) copy-start(bf16[128,128]{1,0:T(8,128)(2,1)} %constant.14.clone.merge_ref) | copy-start | bytes 98308
  0.0 165.4 %copy-start = (bf16[512,2048]{1,0:T(8,128)(2,1)S(1)}, bf16[512,2048]{1,0:T(8,128)(2,1)}, u32[]{:S(2)}) copy-start(bf16[512,2048]{1,0:T(8,128)(2,1)} %w_ref.1) | copy-start | bytes 6291460

commit v7 on v6

--- a/solution.py
+++ b/solution.py
@@ -12,7 +12,7 @@
 GROUP_CH = 128
 NORM_EPS = 1e-06
 CORES = 2
-IN_PARTS = 2
+IN_PARTS = 4
 OUT_PARTS = 4
 VMEM_LIMIT = 16 * 1024 * 1024
 PROJECT_LIMIT = 60 * 1024 * 1024
@@ -64,42 +64,33 @@
     return spread.reshape(high, -1), turns, gather.reshape(CORES, high, -1)
 
 
-def project(tok_hbm, gain_hbm, w_hbm, spread_hbm, out_ref, tok_v, w_v, gain_v, spread_v, sems, small_sems):
+def project(
+    tok_hbm, gain_hbm, w_hbm, spread_hbm, out_ref, tok_v, w_v, gain_v, spread_v, w_sems, sems
+):
     toks, width = tok_v.shape
     part = width // IN_PARTS
-    small = [
-        pltpu.make_async_copy(gain_hbm, gain_v, small_sems.at[0]),
-        pltpu.make_async_copy(spread_hbm, spread_v, small_sems.at[1]),
-    ]
-    copies = []
+    tok_copy = pltpu.make_async_copy(tok_hbm.at[0], tok_v, sems.at[0])
+    gain_copy = pltpu.make_async_copy(gain_hbm, gain_v, sems.at[1])
+    spread_copy = pltpu.make_async_copy(spread_hbm, spread_v, sems.at[2])
+    w_copies = []
     for j in range(IN_PARTS):
         at = pl.ds(j * part, part)
-        copies.append(
-            (
-                pltpu.make_async_copy(tok_hbm.at[0, :, at], tok_v.at[:, at], sems.at[0, j]),
-                pltpu.make_async_copy(w_hbm.at[at, :], w_v.at[at, :], sems.at[1, j]),
-            )
-        )
-    small[0].start()
-    for pair in copies:
-        for copy in pair:
-            copy.start()
-    small[1].start()
-    small[0].wait()
+        w_copies.append(pltpu.make_async_copy(w_hbm.at[at, :], w_v.at[at, :], w_sems.at[j]))
+    for copy in [tok_copy, gain_copy, *w_copies, spread_copy]:
+        copy.start()
+    tok_copy.wait()
+    gain_copy.wait()
+    x = tok_v[...].astype(F32)
     gain = gain_v[...].astype(F32).reshape(1, width)
-    squares = jnp.zeros((toks, 1), F32)
+    factor = lax.rsqrt(jnp.mean(x * x, axis=-1, keepdims=True) + NORM_EPS)
+    tok_v[...] = (x * gain).astype(BF16)
     total = jnp.zeros((toks, w_v.shape[1]), F32)
     for j in range(IN_PARTS):
         at = slice(j * part, (j + 1) * part)
-        copies[j][0].wait()
-        x = tok_v[:, at].astype(F32)
-        squares += jnp.sum(x * x, axis=-1, keepdims=True)
-        scaled = (x * gain[:, at]).astype(BF16)
-        copies[j][1].wait()
-        total += jnp.dot(scaled, w_v[at, :], preferred_element_type=F32)
-    factor = lax.rsqrt(squares * (1.0 / width) + NORM_EPS)
+        w_copies[j].wait()
+        total += jnp.dot(tok_v[:, at], w_v[at, :], preferred_element_type=F32)
     mixin = (total * factor).astype(BF16)
-    small[1].wait()
+    spread_copy.wait()
     for g in range(w_v.shape[1] // GROUP_CH):
         at = slice(g * GROUP_CH, (g + 1) * GROUP_CH)
         out_ref[at, :] = lax.dot_general(
@@ -191,8 +182,8 @@
             pltpu.VMEM((width, feats), BF16),
             pltpu.VMEM(norm_gain.shape, BF16),
             pltpu.VMEM(spread.shape, BF16),
-            pltpu.SemaphoreType.DMA((2, IN_PARTS)),
-            pltpu.SemaphoreType.DMA((2,)),
+            pltpu.SemaphoreType.DMA((IN_PARTS,)),
+            pltpu.SemaphoreType.DMA((3,)),
         ],
         compiler_params=pltpu.CompilerParams(vmem_limit_bytes=PROJECT_LIMIT),
         name="project",

time: 167 us -> 167 us (level)
  no operation moved by 1% of the time
where the time goes in v7:
time: 167 us
  blocking collectives  162 us (97%)
  Pallas kernels  4.41 us (3%)
    all_to_all x2, blocking collectives, exchange(): x = lax.all_to_all(x, ('row', 'y'), split_axis=0, concat_axis=0, tiled=True)  160 us

profile of v7, /device:TPU:6, one launch (start us, length us, event | category | flops | bytes accessed | tf_op | source)
XLA Modules:
  0.0 166.8 jit_solution(7022352420988903196)
XLA Ops:
  0.0 0.0 copy-start.1
  0.0 0.0 copy-start.3
  0.0 0.0 copy-start.2
  0.0 0.0 copy-start.4
  0.0 0.0 copy-start
  0.0 2.5 %project.1 = bf16[512,128]{1,0:T(8,128)(2,1)S(1)} custom-call(bf16[1,128,2048]{2,1,0:T(8,128)(2,1)} %tok_hbm.1, bf16[2048]{0:T(1024)(128)(2,1)} %gain_hbm.1, bf16[2048,512]{1,0:T(8,128)(2,1)} %w_hbm.1, bf16[128,128]{1,0:T(8,128)(2,1)} %constant.10.clone.spread_hbm), custom_call_target="tpu_custom_call" | custom-call | tf_op jit(solution)/shard_map/project/pallas_call | solution.py:175
  2.5 125.1 %all_to_all.10 = bf16[256,2,128]{2,1,0:T(2,128)(2,1)S(1)} all-to-all(bf16[256,2,128]{2,1,0:T(2,128)(2,1)S(1)} %bitcast.8), channel_id=1, replica_groups=mesh['grp'=2,'row'=16,'y'=16,'core'=2] {'row','y'}, dimensions={0} | all-to-all | bytes 262144 | tf_op jit(solution)/shard_map/all_to_all | solution.py:241
  127.6 0.0 copy-done.1
  127.6 0.0 copy-done.3
  127.6 0.3 transform_a.1
  127.9 2.0 %all-gather = bf16[1024,128]{1,0:T(8,128)(2,1)S(1)} all-gather(bf16[512,128]{1,0:T(8,128)(2,1)S(1)} %get-tuple-element.8), channel_id=2, replica_groups=mesh['grp'=2,'row'=16,'y'=16,'core'=2] {'core'}, dimensions={0}, use_global_device_ids=true | all-gather | bytes 393216 | tf_op jit(solution)/shard_map/all_gather | solution.py:246
  130.0 0.0 copy-done.2
  130.0 0.3 transform_b.1
  130.3 35.0 %all_to_all.11 = bf16[256,2,128]{2,1,0:T(2,128)(2,1)S(1)} all-to-all(bf16[256,2,128]{2,1,0:T(2,128)(2,1)S(1)} %bitcast.9), channel_id=1, replica_groups=mesh['grp'=2,'row'=16,'y'=16,'core'=2] {'row','y'}, dimensions={0} | all-to-all | bytes 262144 | tf_op jit(solution)/shard_map/all_to_all | solution.py:241
  165.3 0.0 copy-done.4
  165.3 0.0 copy-done
  165.3 1.3 merge_out.1
Async XLA Ops:
  0.0 127.6 %copy-start.1 = (f32[2,2,2,128,128]{4,3,2,1,0:T(8,128)S(1)}, f32[2,2,2,128,128]{4,3,2,1,0:T(8,128)}, u32[]{:S(2)}) copy-start(f32[2,2,2,128,128]{4,3,2,1,0:T(8,128)} %constant.12.clone.turn_ref) | copy-start | bytes 1572868
  0.0 127.6 %copy-start.3 = (bf16[256,512]{1,0:T(8,128)(2,1)S(1)}, bf16[256,512]{1,0:T(8,128)(2,1)}, u32[]{:S(2)}) copy-start(bf16[256,512]{1,0:T(8,128)(2,1)} %constant.11.clone.first_ref) | copy-start | bytes 786436
  0.0 130.0 %copy-start.2 = (bf16[2,256,256]{2,1,0:T(8,128)(2,1)S(1)}, bf16[2,256,256]{2,1,0:T(8,128)(2,1)}, u32[]{:S(2)}) copy-start(bf16[2,256,256]{2,1,0:T(8,128)(2,1)} %constant.13.clone.last_ref) | copy-start | bytes 786436
  0.0 165.3 %copy-start.4 = (bf16[128,128]{1,0:T(8,128)(2,1)S(1)}, bf16[128,128]{1,0:T(8,128)(2,1)}, u32[]{:S(2)}) copy-start(bf16[128,128]{1,0:T(8,128)(2,1)} %constant.14.clone.merge_ref) | copy-start | bytes 98308
  0.0 165.3 %copy-start = (bf16[512,2048]{1,0:T(8,128)(2,1)S(1)}, bf16[512,2048]{1,0:T(8,128)(2,1)}, u32[]{:S(2)}) copy-start(bf16[512,2048]{1,0:T(8,128)(2,1)} %w_ref.1) | copy-start | bytes 6291460

commit v8 on v7

--- a/solution.py
+++ b/solution.py
@@ -13,7 +13,7 @@
 NORM_EPS = 1e-06
 CORES = 2
 IN_PARTS = 4
-OUT_PARTS = 4
+OUT_SPLIT = (0, 6, 11, 15, 16)
 VMEM_LIMIT = 16 * 1024 * 1024
 PROJECT_LIMIT = 60 * 1024 * 1024
 
@@ -148,18 +148,14 @@
             ).astype(BF16)
         )
     spectrum = jnp.concatenate(pieces, axis=1)
-    part = width // OUT_PARTS
     copies = []
-    for j in range(OUT_PARTS):
-        at = slice(j * part, (j + 1) * part)
-        out_v[:, at] = jnp.dot(spectrum, w_ref[:, at], preferred_element_type=F32).astype(BF16)
-        copies.append(
-            pltpu.make_async_copy(
-                out_v.at[:, pl.ds(j * part, part)],
-                out_hbm.at[0, :, pl.ds(j * part, part)],
-                sems.at[j],
-            )
-        )
+    for j in range(len(OUT_SPLIT) - 1):
+        low, high = (width * cut // OUT_SPLIT[-1] for cut in OUT_SPLIT[j : j + 2])
+        out_v[:, low:high] = jnp.dot(
+            spectrum, w_ref[:, low:high], preferred_element_type=F32
+        ).astype(BF16)
+        at = pl.ds(low, high - low)
+        copies.append(pltpu.make_async_copy(out_v.at[:, at], out_hbm.at[0, :, at], sems.at[j]))
         copies[-1].start()
     for copy in copies:
         copy.wait()
@@ -224,7 +220,7 @@
         out_shape=jax.ShapeDtypeStruct((1, toks, width), BF16),
         in_specs=[VMEM, VMEM, VMEM],
         out_specs=HBM,
-        scratch_shapes=[pltpu.VMEM((toks, width), BF16), pltpu.SemaphoreType.DMA((OUT_PARTS,))],
+        scratch_shapes=[pltpu.VMEM((toks, width), BF16), pltpu.SemaphoreType.DMA((len(OUT_SPLIT) - 1,))],
         compiler_params=pltpu.CompilerParams(vmem_limit_bytes=VMEM_LIMIT),
         name="merge_out",
     )(x, merge, w_out)

time: 167 us -> 167 us (level)
  no operation moved by 1% of the time
where the time goes in v8:
time: 167 us
  blocking collectives  162 us (97%)
  Pallas kernels  4.41 us (3%)
    all_to_all x2, blocking collectives, exchange(): x = lax.all_to_all(x, ('row', 'y'), split_axis=0, concat_axis=0, tiled=True)  160 us

profile of v8, /device:TPU:6, one launch (start us, length us, event | category | flops | bytes accessed | tf_op | source)
XLA Modules:
  0.0 166.8 jit_solution(655270767407019336)
XLA Ops:
  0.0 0.0 copy-start.1
  0.0 0.0 copy-start.3
  0.0 0.0 copy-start.2
  0.0 0.0 copy-start.4
  0.0 0.0 copy-start
  0.0 2.5 %project.1 = bf16[512,128]{1,0:T(8,128)(2,1)S(1)} custom-call(bf16[1,128,2048]{2,1,0:T(8,128)(2,1)} %tok_hbm.1, bf16[2048]{0:T(1024)(128)(2,1)} %gain_hbm.1, bf16[2048,512]{1,0:T(8,128)(2,1)} %w_hbm.1, bf16[128,128]{1,0:T(8,128)(2,1)} %constant.10.clone.spread_hbm), custom_call_target="tpu_custom_call" | custom-call | tf_op jit(solution)/shard_map/project/pallas_call | solution.py:171
  2.5 125.1 %all_to_all.10 = bf16[256,2,128]{2,1,0:T(2,128)(2,1)S(1)} all-to-all(bf16[256,2,128]{2,1,0:T(2,128)(2,1)S(1)} %bitcast.8), channel_id=1, replica_groups=mesh['grp'=2,'row'=16,'y'=16,'core'=2] {'row','y'}, dimensions={0} | all-to-all | bytes 262144 | tf_op jit(solution)/shard_map/all_to_all | solution.py:237
  127.6 0.0 copy-done.1
  127.6 0.0 copy-done.3
  127.6 0.3 transform_a.1
  127.9 2.0 %all-gather = bf16[1024,128]{1,0:T(8,128)(2,1)S(1)} all-gather(bf16[512,128]{1,0:T(8,128)(2,1)S(1)} %get-tuple-element.8), channel_id=2, replica_groups=mesh['grp'=2,'row'=16,'y'=16,'core'=2] {'core'}, dimensions={0}, use_global_device_ids=true | all-gather | bytes 393216 | tf_op jit(solution)/shard_map/all_gather | solution.py:242
  130.0 0.0 copy-done.2
  130.0 0.3 transform_b.1
  130.3 35.0 %all_to_all.11 = bf16[256,2,128]{2,1,0:T(2,128)(2,1)S(1)} all-to-all(bf16[256,2,128]{2,1,0:T(2,128)(2,1)S(1)} %bitcast.9), channel_id=1, replica_groups=mesh['grp'=2,'row'=16,'y'=16,'core'=2] {'row','y'}, dimensions={0} | all-to-all | bytes 262144 | tf_op jit(solution)/shard_map/all_to_all | solution.py:237
  165.3 0.0 copy-done.4
  165.3 0.0 copy-done
  165.3 1.3 merge_out.1
Async XLA Ops:
  0.0 127.6 %copy-start.1 = (f32[2,2,2,128,128]{4,3,2,1,0:T(8,128)S(1)}, f32[2,2,2,128,128]{4,3,2,1,0:T(8,128)}, u32[]{:S(2)}) copy-start(f32[2,2,2,128,128]{4,3,2,1,0:T(8,128)} %constant.12.clone.turn_ref) | copy-start | bytes 1572868
  0.0 127.6 %copy-start.3 = (bf16[256,512]{1,0:T(8,128)(2,1)S(1)}, bf16[256,512]{1,0:T(8,128)(2,1)}, u32[]{:S(2)}) copy-start(bf16[256,512]{1,0:T(8,128)(2,1)} %constant.11.clone.first_ref) | copy-start | bytes 786436
  0.0 130.0 %copy-start.2 = (bf16[2,256,256]{2,1,0:T(8,128)(2,1)S(1)}, bf16[2,256,256]{2,1,0:T(8,128)(2,1)}, u32[]{:S(2)}) copy-start(bf16[2,256,256]{2,1,0:T(8,128)(2,1)} %constant.13.clone.last_ref) | copy-start | bytes 786436
  0.0 165.3 %copy-start.4 = (bf16[128,128]{1,0:T(8,128)(2,1)S(1)}, bf16[128,128]{1,0:T(8,128)(2,1)}, u32[]{:S(2)}) copy-start(bf16[128,128]{1,0:T(8,128)(2,1)} %constant.14.clone.merge_ref) | copy-start | bytes 98308
  0.0 165.3 %copy-start = (bf16[512,2048]{1,0:T(8,128)(2,1)S(1)}, bf16[512,2048]{1,0:T(8,128)(2,1)}, u32[]{:S(2)}) copy-start(bf16[512,2048]{1,0:T(8,128)(2,1)} %w_ref.1) | copy-start | bytes 6291460
